TPU v7x, 32 devices: a whole 2x2x4 slice. The times are simulated.
32 devices in a mesh: sp: 8 (over z, y), tp: 4 (over x, core).
Axes of the slice: x: 2, y: 2, z: 4, core: 2. Of those that a mesh axis runs over, the one named last changes fastest.
Arguments:
- cotangent: bfloat16 [1024, 2048], P('sp', 'tp'), may hold values from -6 to 6
- mixer_out: bfloat16 [1024, 2048], P('sp', 'tp'), may hold values from -6 to 6
- route_ids: int32 [1024, 2], P('sp'), may hold values from 0 to 7, all different within a row; in each aligned block of 128 rows (0 to 127, 128 to 255, ...) at most 64 rows name the same one
- route_weights: float32 [1024, 2], P('sp'), may hold values from 0.2 to 1
- conv_out: bfloat16 [1024, 2048], P('sp', 'tp'), may hold values from -6 to 6
- recur_gate: bfloat16 [1024, 2048], P('sp', 'tp'), may hold values from 0.007 to 1
- input_gate: bfloat16 [1024, 2048], P('sp', 'tp'), may hold values from 0.099609375 to 0.8984375
- gate_pre: bfloat16 [1024, 2048], P('sp', 'tp'), may hold values from -6 to 6
- states_before: bfloat16 [1024, 2048], P('sp', 'tp'), may hold values from -4 to 4
- decay_rate: float32 [2048], P('tp'), may hold values from 4e-07 to 0.008
- out_proj: bfloat16 [2048, 2048], P(None, 'tp'), may hold values from -0.125 to 0.125
- recur_map: bfloat16 [4, 512, 512], P('tp'), may hold values from -0.25 to 0.25
- input_map: bfloat16 [4, 512, 512], P('tp'), may hold values from -0.25 to 0.25
- expert_gate: bfloat16 [8, 2048, 1024], P('sp', None, 'tp'), may hold values from -0.125 to 0.125
- expert_up: bfloat16 [8, 2048, 1024], P('sp', None, 'tp'), may hold values from -0.125 to 0.125
- expert_down: bfloat16 [8, 1024, 2048], P('sp', 'tp'), may hold values from -0.1875 to 0.1875
Outputs:
- grad_expert_gate: bfloat16 [8, 2048, 1024], P('sp', None, 'tp')
- grad_expert_up: bfloat16 [8, 2048, 1024], P('sp', None, 'tp')
- grad_expert_down: bfloat16 [8, 1024, 2048], P('sp', 'tp')
- grad_out_proj: float32 [2048, 2048], P('sp', 'tp')
- grad_conv: bfloat16 [1024, 2048], P('sp', 'tp')
- grad_gate_pre: bfloat16 [1024, 2048], P('sp', 'tp')
Inputs may be any that keep to these rules, and one draw needn't show every extreme that they name: `route_ids`: the two experts of a token differ. In every aligned block of 128 tokens no expert is named by more than 64 routes, and in some block some expert by exactly 64.
All inputs are finite; a program needn't handle non-finite values.
Results may differ from a plain program's by a relative error of at most 0.0093.
Values may be sent and summed in bfloat16 or wider, within the bound.
No kernel may reach another device: no remote copies, remote signals or barrier semaphores. Data moves between devices by JAX's collectives and lax.ppermute only.
A program may use at most 64 MiB of HBM per device.

v0:
```python
import functools

import jax
import jax.numpy as jnp
from jax import lax
from jax.experimental import pallas as pl
from jax.experimental.pallas import tpu as pltpu
from jax.sharding import PartitionSpec as P


BF = jnp.bfloat16
F32 = jnp.float32
VM = pl.BlockSpec(memory_space=pltpu.VMEM)
ANY = pl.BlockSpec(memory_space=pl.ANY)
HB = pl.BlockSpec(memory_space=pltpu.HBM)


def hop(value, axis, bit):
    count = lax.axis_size(axis)
    return lax.ppermute(value, axis, [(i, i ^ bit) for i in range(count)])


def dot(left, right):
    return jnp.dot(left, right, preferred_element_type=F32)


def dot_nt(left, right):
    return lax.dot_general(left, right, (((1,), (1,)), ((), ())), preferred_element_type=F32)


def dot_tn(left, right):
    return lax.dot_general(left, right, (((0,), (0,)), ((), ())), preferred_element_type=F32)


def call(kernel, outs, ins, specs, flops, scratch=(), limit=8):
    nbytes = sum(a.size * a.dtype.itemsize for a in list(outs) + list(ins))
    return pl.pallas_call(
        kernel,
        out_shape=list(outs),
        in_specs=specs,
        out_specs=[VM] * len(outs),
        scratch_shapes=list(scratch),
        compiler_params=pltpu.CompilerParams(vmem_limit_bytes=limit * 2**20),
        cost_estimate=pl.CostEstimate(flops=flops, bytes_accessed=nbytes, transcendentals=0),
    )(*ins)


def struct(shape, dtype):
    return jax.ShapeDtypeStruct(shape, dtype)


def dispatch_kernel(n, cap, *refs):
    d_ref, first_ref, blocks = refs[4], refs[5], refs[6 : 6 + n]
    held, sems = refs[6 + n : 10 + n], refs[10 + n]
    me = lax.axis_index("sp")
    copies = [pltpu.make_async_copy(refs[i], held[i], sems.at[i]) for i in range(4)]
    for copy in copies:
        copy.start()
    for copy in copies:
        copy.wait()
    ids_ref, w_ref, x_ref, g_ref = held
    tok, feat = x_ref.shape
    ids = ids_ref[...] ^ me
    who = lax.broadcasted_iota(jnp.int32, (n, tok), 0)
    earlier = (
        lax.broadcasted_iota(jnp.int32, (tok, tok), 0)
        < lax.broadcasted_iota(jnp.int32, (tok, tok), 1)
    )
    earlier = jnp.where(earlier, 1.0, 0.0).astype(BF)
    one = [jnp.where(who == ids[k : k + 1, :], 1.0, 0.0) for k in range(2)]
    before = [dot(o.astype(BF), earlier) for o in one]
    before[1] = before[1] + jnp.sum(one[0], axis=1, keepdims=True)
    rank = [jnp.sum(b * o, axis=0, keepdims=True) for b, o in zip(before, one)]
    pos = [ids[k : k + 1, :] * cap + rank[k].astype(jnp.int32) for k in range(2)]
    slot = lax.broadcasted_iota(jnp.int32, (n * cap, tok), 0)
    hit = [slot == p for p in pos]
    weight = jnp.where(hit[0], w_ref[0:1, :], 0.0) + jnp.where(hit[1], w_ref[1:2, :], 0.0)
    weight = jnp.sum(weight, axis=1, keepdims=True)
    pick = jnp.where(hit[0] | hit[1], 1.0, 0.0).astype(BF)
    d_ref[...] = pick
    row = lax.broadcasted_iota(jnp.int32, first_ref.shape, 0)
    first_ref[...] = jnp.where((row == 0) & (me == 0), 1.0, 0.0)
    rows = dot(pick, x_ref[...]).astype(BF)
    cots = (dot(pick, g_ref[...]) * weight).astype(BF)
    for k, block in enumerate(blocks):
        block[:, :feat] = rows[k * cap : (k + 1) * cap]
        block[:, feat:] = cots[k * cap : (k + 1) * cap]


def expert_kernel(m, *refs):
    me = lax.axis_index("tp")
    parts, (wg_ref, wu_ref, wd_ref) = refs[:m], refs[m : m + 3]
    dg_ref, du_ref, act_ref, keep_ref, send_ref = refs[-5:]
    feat = parts[0].shape[1] // 2

    def span(q):
        return pl.ds(pl.multiple_of((me ^ q) * feat, feat), feat)

    pre_gate = pre_up = d_active = 0.0
    for q in range(m):
        rows = parts[q][:, :feat]
        pre_gate += dot(rows, wg_ref[span(q), :])
        pre_up += dot(rows, wu_ref[span(q), :])
        d_active += dot_nt(parts[q][:, feat:], wd_ref[:, span(q)])
    sig = jax.nn.sigmoid(pre_gate)
    gate_act = pre_gate * sig
    act_ref[...] = (gate_act * pre_up).astype(BF)
    d_gate = (d_active * pre_up * sig * (1.0 + pre_gate * (1.0 - sig))).astype(BF)
    d_up = (d_active * gate_act).astype(BF)
    dg_ref[...] = d_gate
    du_ref[...] = d_up
    for q in range(m):
        part = dot_nt(d_gate, wg_ref[span(q), :]) + dot_nt(d_up, wu_ref[span(q), :])
        target = send_ref if q & 1 else keep_ref
        target[:, (q >> 1) * feat : ((q >> 1) + 1) * feat] = part.astype(BF)


def weight_kernel(m, chunks, *refs):
    me = lax.axis_index("tp")
    parts = [refs[h * m : (h + 1) * m] for h in range(chunks)]
    grads = refs[chunks * m : chunks * (m + 3)]
    gg_ref, gu_ref, gd_ref = refs[-3:]
    feat = parts[0][0].shape[1] // 2
    for q in range(m):
        span = pl.ds(pl.multiple_of((me ^ q) * feat, feat), feat)
        gate = up = down = 0.0
        for h in range(chunks):
            rows = parts[h][q][:, :feat]
            gate += dot_tn(rows, grads[3 * h][...])
            up += dot_tn(rows, grads[3 * h + 1][...])
            down += dot_tn(grads[3 * h + 2][...], parts[h][q][:, feat:])
        gg_ref[span, :] = gate.astype(BF)
        gu_ref[span, :] = up.astype(BF)
        gd_ref[:, span] = down.astype(BF)


def join_kernel(*refs):
    rows = refs[0].shape[0]
    for i, ref in enumerate(refs[:-1]):
        refs[-1][i * rows : (i + 1) * rows, :] = ref[...]


def halve_kernel(feat, keep_ref, got_ref, stay_ref, go_ref):
    count = keep_ref.shape[1] // feat
    for i in range(count):
        cols = slice(i * feat, (i + 1) * feat)
        part = keep_ref[:, cols].astype(F32) + got_ref[:, cols].astype(F32)
        at = slice((i >> 1) * feat, ((i >> 1) + 1) * feat)
        target = go_ref if i & 1 else stay_ref
        target[:, at] = part.astype(target.dtype)


def finish_kernel(cap, keep_ref, got_ref, *outs):
    total = (keep_ref[...].astype(F32) + got_ref[...].astype(F32)).astype(BF)
    for k, out in enumerate(outs):
        out[...] = total[k * cap : (k + 1) * cap]


def combine_kernel(n, cap, d_ref, cot_ref, *refs):
    blocks, out_ref, held = refs[:n], refs[-2], refs[-1]
    for k in range(n):
        held[k * cap : (k + 1) * cap, :] = blocks[k][...]
    out_ref[...] = (dot_tn(d_ref[...], held[...]) + cot_ref[...].astype(F32)).astype(BF)


def recur_kernel(n, m, *refs):
    grads, (op_ref, gate_ref, slope_ref, decay_ref) = refs[:m], refs[m : m + 4]
    dgp_ref, local_ref, weight_ref, send_ref, full_ref = refs[m + 4 :]
    me = lax.axis_index("tp")
    tok, channels = decay_ref.shape
    feat = full_ref.shape[2]
    half, width = tok // 2, send_ref.shape[2]
    total = 0.0
    for q in range(m):
        at = me ^ q
        piece = grads[q][...]
        full_ref[at] = piece
        total += dot(piece, op_ref[pl.ds(pl.multiple_of(at * feat, feat), feat), :])
    dgp_ref[...] = (total * slope_ref[...]).astype(BF)
    value = total * gate_ref[...]
    decay = decay_ref[...]
    first = decay[0:1]
    weight = jnp.concatenate([decay[1:], jnp.ones((1, channels), F32)], axis=0)
    step = 1
    while step < tok:
        pad = jnp.zeros((step, channels), F32)
        value = value + weight * jnp.concatenate([value[step:], pad], axis=0)
        weight = weight * jnp.concatenate([weight[step:], pad + 1.0], axis=0)
        step *= 2
    local_ref[...] = value
    weight_ref[...] = weight
    rows = []
    for edge in (first * weight[0:1], first * value[0:1]):
        high = edge.astype(BF).astype(F32)
        for part in (high, edge - high):
            rows += [part[:, i : i + width] for i in range(0, channels, width)]
    spare = send_ref.shape[1] - half - len(rows)
    if spare:
        rows.append(jnp.zeros((spare, width), F32))
    tail = jnp.concatenate(rows, axis=0).astype(BF)
    own = pl.ds(pl.multiple_of((me & 1) * half, half), half)
    for s in range(n):
        at, col = divmod(s * width, feat)
        send_ref[s, :half, :] = full_ref[at, own, col : col + width]
        send_ref[s, half:, :] = tail


def final_kernel(n, half, local_ref, weight_ref, got_ref, c1_ref, c2_ref, c3_ref, rm_ref,
                 im_ref, out_ref):
    me = lax.axis_index("sp")
    channels, width = local_ref.shape[1], got_ref.shape[2]
    per = channels // width

    def lap(i, incoming):
        s = n - 1 - i
        tail = got_ref[s, half:, :].astype(F32)
        part = [
            jnp.concatenate([tail[p * per + i : p * per + i + 1] for i in range(per)], axis=1)
            for p in range(4)
        ]
        longer = (part[2] + part[3]) + (part[0] + part[1]) * incoming
        return jnp.where(s > me, longer, incoming)

    incoming = lax.fori_loop(0, n - 1, lap, jnp.zeros((1, channels), F32), unroll=n <= 8)
    grad = local_ref[...] + weight_ref[...] * incoming
    d_recur = (grad * c1_ref[...]).astype(BF)
    d_input = (grad * c2_ref[...]).astype(BF)
    groups, width = rm_ref.shape[0], rm_ref.shape[1]
    base = grad * c3_ref[...]
    for b in range(groups):
        cols = slice(b * width, (b + 1) * width)
        part = dot_nt(d_recur[:, cols], rm_ref[b]) + dot_nt(d_input[:, cols], im_ref[b])
        out_ref[:, cols] = (base[:, cols] + part).astype(BF)


def out_proj_kernel(n, tok, orders, own_ref, other_ref, *refs):
    pieces, out_ref, held = refs[: len(orders)], refs[-2], refs[-1]
    half = tok // 2
    me, side = lax.axis_index("sp"), lax.axis_index("tp") & 1
    for piece, order in zip(pieces, orders):
        for i, k in enumerate(order):
            held[me ^ k] = piece[i * tok : (i + 1) * tok]
    total = 0.0
    for s in range(n):
        for part, bit in ((own_ref, 0), (other_ref, 1)):
            at = pl.ds(pl.multiple_of((side ^ bit) * half, half), half)
            total += dot_tn(part[s, :half, :], held[s, at, :])
    out_ref[...] = total


def body(
    cotangent,
    mixer_out,
    route_ids,
    route_weights,
    conv_out,
    recur_gate,
    input_gate,
    gate_pre,
    states_before,
    decay_rate,
    out_proj,
    recur_map,
    input_map,
    expert_gate,
    expert_up,
    expert_down,
):
    tok, feat = cotangent.shape
    n, m = lax.axis_size("sp"), lax.axis_size("tp")
    cap = 4 * tok // n
    slots = n * cap
    wg, wu, wd = expert_gate[0], expert_up[0], expert_down[0]
    hidden = wg.shape[1]
    channels = conv_out.shape[1]

    sent = call(
        functools.partial(dispatch_kernel, n, cap),
        [struct((slots, tok), BF), struct((tok, 128), F32)] + [struct((cap, 2 * feat), BF)] * n,
        [route_ids.T, route_weights.T, mixer_out, cotangent],
        [HB] * 4,
        4 * slots * tok * feat,
        scratch=[
            pltpu.VMEM((2, tok), jnp.int32),
            pltpu.VMEM((2, tok), F32),
            pltpu.VMEM((tok, feat), BF),
            pltpu.VMEM((tok, feat), BF),
            pltpu.SemaphoreType.DMA((4,)),
        ],
    )
    pick, first, sent = sent[0], sent[1], sent[2:]
    edges = [0, 1, n // 2, 3 * n // 4, n]
    chunks = [range(a, b) for a, b in zip(edges, edges[1:])]
    got = [sent[0]] + [hop(sent[k], "sp", k) for k in range(1, n)]

    rate = decay_rate[None, :]
    recur_f = recur_gate.astype(F32)
    input_f = input_gate.astype(F32)
    conv_f = conv_out.astype(F32)
    before_f = states_before.astype(F32)
    log_decay = -8.0 * recur_f * rate
    decay_now = jnp.exp(log_decay)
    at_start = first[:, :1] > 0.5
    norm_factor = jnp.where(at_start, 1.0, jnp.sqrt(-jnp.expm1(2.0 * log_decay)))
    norm_slope = jnp.where(at_start, 0.0, -jnp.exp(2.0 * log_decay) / norm_factor)
    drive = input_f * conv_f
    kept = decay_now * before_f
    state = kept + norm_factor * drive
    gate, gelu_back = jax.vjp(jax.nn.gelu, gate_pre.astype(F32))
    slope = gelu_back(state)[0]
    mixed = (state * gate).astype(BF)
    c1 = (kept + norm_slope * drive) * (-8.0 * rate) * recur_f * (1.0 - recur_f)
    c3 = norm_factor * input_f
    c2 = c3 * conv_f * (1.0 - input_f)

    parts, grads, back = [], [], [None] * n
    before = []
    for chunk in chunks:
        rows = len(chunk) * cap
        joined = call(
            join_kernel,
            [struct((rows, 2 * feat), BF)],
            [got[k] for k in chunk],
            [VM] * len(chunk),
            rows * feat,
        )
        here = {0: joined[0]}
        if chunk is chunks[-1]:
            pieces, orders = [mixed, hop(mixed, "sp", n // 2)], [[0], [n // 2]]
        bit = m // 2
        while bit:
            for q in sorted(here):
                here[q | bit] = hop(here[q], "tp", bit)
            bit //= 2
        piece = [here[q] for q in range(m)]
        d_gate, d_up, active, keep, give = call(
            functools.partial(expert_kernel, m),
            [struct((rows, hidden), BF)] * 3 + [struct((rows, m * feat // 2), BF)] * 2,
            piece + [wg, wu, wd] + before,
            [VM] * (m + 3) + [ANY] * len(before),
            10 * rows * m * feat * hidden,
            limit=16,
        )
        before = [d_up]
        parts.append(piece)
        grads.append([d_gate, d_up, active])
        bit = 1
        while 2 * bit < m:
            keep, give = call(
                functools.partial(halve_kernel, feat),
                [struct((rows, keep.shape[1] // 2), t) for t in (F32, BF)],
                [keep, hop(give, "tp", bit)],
                [VM, VM],
                rows * m * feat,
            )
            bit *= 2
        blocks = call(
            functools.partial(finish_kernel, cap),
            [struct((cap, feat), BF)] * len(chunk),
            [keep, hop(give, "tp", bit)],
            [VM, VM],
            rows * feat,
        )
        for k, block in zip(chunk, blocks):
            back[k] = hop(block, "sp", k) if k else block

    bit = n // 4
    while bit:
        stacked = jnp.concatenate(pieces, axis=0)
        order = [k for group in orders for k in group]
        pieces.append(hop(stacked, "sp", bit))
        orders.append([k | bit for k in order])
        bit //= 2

    grad_gate, grad_up, grad_down = call(
        functools.partial(weight_kernel, m, len(chunks)),
        [struct(wg.shape, BF), struct(wu.shape, BF), struct(wd.shape, BF)],
        [a for piece in parts for a in piece] + [a for g in grads for a in g],
        [VM] * (len(chunks) * (m + 3)),
        6 * slots * m * feat * hidden,
        limit=24,
    )

    out_grad = {
        0: call(
            functools.partial(combine_kernel, n, cap),
            [struct((tok, feat), BF)],
            [pick, cotangent, *back],
            [VM] * (n + 2),
            2 * slots * tok * feat,
            scratch=[pltpu.VMEM((slots, feat), BF)],
        )[0]
    }
    bit = m // 2
    while bit:
        for q in sorted(out_grad):
            out_grad[q | bit] = hop(out_grad[q], "tp", bit)
        bit //= 2

    half, width = tok // 2, m * feat // n
    spare = -(-4 * channels // width // 16) * 16
    grad_gate_pre, local_grad, carry_weight, slices = call(
        functools.partial(recur_kernel, n, m),
        [struct((tok, channels), BF)]
        + [struct((tok, channels), F32)] * 2
        + [struct((n, half + spare, width), BF)],
        [*[out_grad[q] for q in range(m)], out_proj, gate, slope, decay_now],
        [VM] * (m + 4),
        2 * tok * m * feat * channels,
        scratch=[pltpu.VMEM((m, tok, feat), BF)],
    )
    own = lax.all_to_all(slices, "sp", split_axis=0, concat_axis=0, tiled=True)
    other = hop(own, "tp", 1)
    grad_conv = call(
        functools.partial(final_kernel, n, half),
        [struct((tok, channels), BF)],
        [local_grad, carry_weight, own, c1, c2, c3, recur_map, input_map],
        [VM] * 8,
        4 * tok * channels * recur_map.shape[1],
    )[0]
    grad_out_proj = call(
        functools.partial(out_proj_kernel, n, tok, orders),
        [struct((width, channels), F32)],
        [own, other, *pieces],
        [VM] * (2 + len(pieces)),
        2 * n * tok * width * channels,
        scratch=[pltpu.VMEM((n, tok, channels), BF)],
        limit=32 if n > 8 else 8,
    )[0]
    return (
        grad_gate[None],
        grad_up[None],
        grad_down[None],
        grad_out_proj,
        grad_conv,
        grad_gate_pre,
    )


def solution(mesh):
    placed = (
        P("sp", "tp"),
        P("sp", "tp"),
        P("sp", None),
        P("sp", None),
        P("sp", "tp"),
        P("sp", "tp"),
        P("sp", "tp"),
        P("sp", "tp"),
        P("sp", "tp"),
        P("tp"),
        P(None, "tp"),
        P("tp", None, None),
        P("tp", None, None),
        P("sp", None, "tp"),
        P("sp", None, "tp"),
        P("sp", "tp", None),
    )

    return jax.shard_map(
        body,
        mesh=mesh,
        in_specs=placed,
        out_specs=(
            P("sp", None, "tp"),
            P("sp", None, "tp"),
            P("sp", "tp", None),
            P("sp", "tp"),
            P("sp", "tp"),
            P("sp", "tp"),
        ),
        check_vma=False,
    )
```

profile of v0, /device:TPU:0, one launch (start us, length us, event | category | flops | bytes accessed | tf_op | source)
XLA Modules:
  0.0 148.9 jit_solution(31264904614791765)
XLA Ops:
  5.0 3.1 %collective-permute-start.3 = (bf16[64,1024]{1,0:T(8,128)(2,1)S(1)}, bf16[64,1024]{1,0:T(8,128)(2,1)S(1)}, u32[]{:S(2)}, u32[]{:S(2)}) collective-permute-start(bf16[64,1024]{1,0:T(8,128)(2,1)S(1)} %get-tuple-element.59), channel_id=1, source_target_pairs={{0,4},{4,0},{8,12},{12,8},{16,20},{20,16},{24,28},{28,24},{1,5},{5... | collective-permute-start | bytes 393224 | tf_op jit(solution)/shard_map/ppermute | solution.py:20
  9.6 1.9 %collective-permute-done.3.refs_0_ = bf16[64,1024]{1,0:T(8,128)(2,1)S(1)} collective-permute-done((bf16[64,1024]{1,0:T(8,128)(2,1)S(1)}, bf16[64,1024]{1,0:T(8,128)(2,1)S(1)}, u32[]{:S(2)}, u32[]{:S(2)}) %collective-permute-start.3) | collective-permute-done | bytes 131104 | tf_op jit(solution)/shard_map/ppermute | solution.py:20
  11.5 2.9 %collective-permute-done.4.refs_1_ = bf16[64,1024]{1,0:T(8,128)(2,1)S(1)} collective-permute-done((bf16[64,1024]{1,0:T(8,128)(2,1)S(1)}, bf16[64,1024]{1,0:T(8,128)(2,1)S(1)}, u32[]{:S(2)}, u32[]{:S(2)}) %collective-permute-start.4) | collective-permute-done | bytes 131104 | tf_op jit(solution)/shard_map/ppermute | solution.py:20
  17.3 3.5 %collective-permute-start.10 = (bf16[64,1024]{1,0:T(8,128)(2,1)S(1)}, bf16[64,1024]{1,0:T(8,128)(2,1)S(1)}, u32[]{:S(2)}, u32[]{:S(2)}) collective-permute-start(bf16[64,1024]{1,0:T(8,128)(2,1)S(1)} %get-tuple-element.63), channel_id=1, source_target_pairs={{0,20},{4,16},{8,28},{12,24},{16,4},{20,0},{24,12},{28,8},{1,21},{... | collective-permute-start | bytes 393224 | tf_op jit(solution)/shard_map/ppermute | solution.py:20
  21.2 3.6 %collective-permute-start.14 = (bf16[64,1024]{1,0:T(8,128)(2,1)S(1)}, bf16[64,1024]{1,0:T(8,128)(2,1)S(1)}, u32[]{:S(2)}, u32[]{:S(2)}) collective-permute-start(bf16[64,1024]{1,0:T(8,128)(2,1)S(1)} %get-tuple-element.64), channel_id=1, source_target_pairs={{0,24},{4,28},{8,16},{12,20},{16,8},{20,12},{24,0},{28,4},{1,25},{... | collective-permute-start | bytes 393224 | tf_op jit(solution)/shard_map/ppermute | solution.py:20
  25.0 10.3 %collective-permute-done.10.refs_1_ = bf16[64,1024]{1,0:T(8,128)(2,1)S(1)} collective-permute-done((bf16[64,1024]{1,0:T(8,128)(2,1)S(1)}, bf16[64,1024]{1,0:T(8,128)(2,1)S(1)}, u32[]{:S(2)}, u32[]{:S(2)}) %collective-permute-start.10) | collective-permute-done | bytes 131104 | tf_op jit(solution)/shard_map/ppermute | solution.py:20
  35.7 2.5 %collective-permute-done.9.refs_0_ = bf16[64,1024]{1,0:T(8,128)(2,1)S(1)} collective-permute-done((bf16[64,1024]{1,0:T(8,128)(2,1)S(1)}, bf16[64,1024]{1,0:T(8,128)(2,1)S(1)}, u32[]{:S(2)}, u32[]{:S(2)}) %collective-permute-start.9) | collective-permute-done | bytes 131104 | tf_op jit(solution)/shard_map/ppermute | solution.py:20
  42.5 5.5 %collective-permute-done.12.refs_2_.refs_10_ = bf16[128,1024]{1,0:T(8,128)(2,1)S(1)} collective-permute-done((bf16[128,1024]{1,0:T(8,128)(2,1)S(1)}, bf16[128,1024]{1,0:T(8,128)(2,1)S(1)}, u32[]{:S(2)}, u32[]{:S(2)}) %collective-permute-start.12) | collective-permute-done | bytes 262176 | tf_op jit(solution)/shard_map/ppermute | solution.py:20
  48.0 4.6 %collective-permute-done.17.refs_2_.refs_14_ = bf16[128,1024]{1,0:T(8,128)(2,1)S(1)} collective-permute-done((bf16[128,1024]{1,0:T(8,128)(2,1)S(1)}, bf16[128,1024]{1,0:T(8,128)(2,1)S(1)}, u32[]{:S(2)}, u32[]{:S(2)}) %collective-permute-start.17) | collective-permute-done | bytes 262176 | tf_op jit(solution)/shard_map/ppermute | solution.py:20
  54.4 1.9 %shard_map.204 = (bf16[64,256]{1,0:T(8,128)(2,1)S(1)}, bf16[64,256]{1,0:T(8,128)(2,1)S(1)}, bf16[64,256]{1,0:T(8,128)(2,1)S(1)}, bf16[64,1024]{1,0:T(8,128)(2,1)S(1)}, bf16[64,1024]{1,0:T(8,128)(2,1)S(1)}) custom-call(bf16[64,1024]{1,0:T(8,128)(2,1)S(1)} %shard_map.200.refs_0_, bf16[64,1024]{1,0:T(8,128)(2,1)S(1)} %collective-permute-done.refs_1_, ...), custom_call_target="tpu_custom_call" | custom-call | flops 335544320 | bytes 4030464 | tf_op jit(solution)/shard_map/pallas_call | solution.py:37
  57.0 2.1 %shard_map.205 = (bf16[192,256]{1,0:T(8,128)(2,1)S(1)}, bf16[192,256]{1,0:T(8,128)(2,1)S(1)}, bf16[192,256]{1,0:T(8,128)(2,1)S(1)}, bf16[192,1024]{1,0:T(8,128)(2,1)S(1)}, bf16[192,1024]{1,0:T(8,128)(2,1)S(1)}) custom-call(bf16[192,1024]{1,0:T(8,128)(2,1)S(1)} %shard_map.201.refs_0_.refs_4_, bf16[192,1024]{1,0:T(8,128)(2,1)S(1)} %collective-permute-done.6.refs_1_.refs_5_, ...), custom_call_target="tpu_custom_call" | custom-call | flops 1006632960 | bytes 5832704 | tf_op jit(solution)/shard_map/pallas_call | solution.py:37
  60.4 1.9 %shard_map.206 = (bf16[128,256]{1,0:T(8,128)(2,1)S(1)}, bf16[128,256]{1,0:T(8,128)(2,1)S(1)}, bf16[128,256]{1,0:T(8,128)(2,1)S(1)}, bf16[128,1024]{1,0:T(8,128)(2,1)S(1)}, bf16[128,1024]{1,0:T(8,128)(2,1)S(1)}) custom-call(bf16[128,1024]{1,0:T(8,128)(2,1)S(1)} %shard_map.202.refs_0_.refs_8_, bf16[128,1024]{1,0:T(8,128)(2,1)S(1)} %collective-permute-done.11.refs_1_.refs_9_, ...), custom_call_target="tpu_custom_call" | custom-call | flops 671088640 | bytes 5013504 | tf_op jit(solution)/shard_map/pallas_call | solution.py:37
  62.5 1.9 %shard_map.207 = (bf16[128,256]{1,0:T(8,128)(2,1)S(1)}, bf16[128,256]{1,0:T(8,128)(2,1)S(1)}, bf16[128,256]{1,0:T(8,128)(2,1)S(1)}, bf16[128,1024]{1,0:T(8,128)(2,1)S(1)}, bf16[128,1024]{1,0:T(8,128)(2,1)S(1)}) custom-call(bf16[128,1024]{1,0:T(8,128)(2,1)S(1)} %shard_map.203.refs_0_.refs_12_, bf16[128,1024]{1,0:T(8,128)(2,1)S(1)} %collective-permute-done.16.refs_1_.refs_13_, ...), custom_call_target="tpu_custom_call" | custom-call | flops 671088640 | bytes 4980736 | tf_op jit(solution)/shard_map/pallas_call | solution.py:37
  70.7 3.1 %collective-permute-done.31.got_ref = bf16[128,512]{1,0:T(8,128)(2,1)S(1)} collective-permute-done((bf16[128,512]{1,0:T(8,128)(2,1)S(1)}, bf16[128,512]{1,0:T(8,128)(2,1)S(1)}, u32[]{:S(2)}, u32[]{:S(2)}) %collective-permute-start.31) | collective-permute-done | bytes 131104 | tf_op jit(solution)/shard_map/ppermute | solution.py:20
  73.8 2.2 %collective-permute-start.32 = (bf16[64,512]{1,0:T(8,128)(2,1)S(1)}, bf16[64,512]{1,0:T(8,128)(2,1)S(1)}, u32[]{:S(2)}, u32[]{:S(2)}) collective-permute-start(bf16[64,512]{1,0:T(8,128)(2,1)S(1)} %get-tuple-element.103), channel_id=1, source_target_pairs={{0,24},{4,28},{8,16},{12,20},{16,8},{20,12},{24,0},{28,4},{1,25},{... | collective-permute-start | bytes 196616 | tf_op jit(solution)/shard_map/ppermute | solution.py:20
  78.3 5.5 %collective-permute-start.28 = (bf16[64,512]{1,0:T(8,128)(2,1)S(1)}, bf16[64,512]{1,0:T(8,128)(2,1)S(1)}, u32[]{:S(2)}, u32[]{:S(2)}) collective-permute-start(bf16[64,512]{1,0:T(8,128)(2,1)S(1)} %get-tuple-element.97), channel_id=1, source_target_pairs={{0,16},{4,20},{8,24},{12,28},{16,0},{20,4},{24,8},{28,12},{1,17},{... | collective-permute-start | bytes 196616 | tf_op jit(solution)/shard_map/ppermute | solution.py:20
  83.8 4.7 %collective-permute-start.29 = (bf16[64,512]{1,0:T(8,128)(2,1)S(1)}, bf16[64,512]{1,0:T(8,128)(2,1)S(1)}, u32[]{:S(2)}, u32[]{:S(2)}) collective-permute-start(bf16[64,512]{1,0:T(8,128)(2,1)S(1)} %get-tuple-element.98), channel_id=1, source_target_pairs={{0,20},{4,16},{8,28},{12,24},{16,4},{20,0},{24,12},{28,8},{1,21},{... | collective-permute-start | bytes 196616 | tf_op jit(solution)/shard_map/ppermute | solution.py:20
  98.7 2.2 %collective-permute-done.35.refs_2_ = bf16[128,512]{1,0:T(8,128)(2,1)S(1)} collective-permute-done((bf16[128,512]{1,0:T(8,128)(2,1)S(1)}, bf16[128,512]{1,0:T(8,128)(2,1)S(1)}, u32[]{:S(2)}, u32[]{:S(2)}) %collective-permute-start.35) | collective-permute-done | bytes 131104 | tf_op jit(solution)/shard_map/ppermute | solution.py:20
  100.9 2.1 %collective-permute-done.38.refs_1_ = bf16[128,512]{1,0:T(8,128)(2,1)S(1)} collective-permute-done((bf16[128,512]{1,0:T(8,128)(2,1)S(1)}, bf16[128,512]{1,0:T(8,128)(2,1)S(1)}, u32[]{:S(2)}, u32[]{:S(2)}) %collective-permute-start.38) | collective-permute-done | bytes 131104 | tf_op jit(solution)/shard_map/ppermute | solution.py:20
  103.8 2.2 %collective-permute-start.39 = (bf16[256,512]{1,0:T(8,128)(2,1)}, bf16[256,512]{1,0:T(8,128)(2,1)S(1)}, u32[]{:S(2)}, u32[]{:S(2)}) collective-permute-start(bf16[256,512]{1,0:T(8,128)(2,1)} %pad_maximum_fusion.1), channel_id=1, source_target_pairs={{0,8},{4,12},{8,0},{12,4},{16,24},{20,28},{24,16},{28,20},{1,9},{5... | collective-permute-start | bytes 786440 | tf_op jit(solution)/shard_map/ppermute | solution.py:20
  108.2 3.6 %all-to-all-start = ((bf16[8,80,256]{2,1,0:T(8,128)(2,1)}), bf16[8,80,256]{2,1,0:T(8,128)(2,1)S(1)}, u32[]{:S(2)}, u32[]{:S(2)}) async-start(bf16[8,80,256]{2,1,0:T(8,128)(2,1)} %get-tuple-element.106), calls=%async_computation | async-start | bytes 655360 | tf_op jit(solution)/shard_map/all_to_all | solution.py:412
  114.4 6.5 %all-to-all-done.own_ref.got_ref = bf16[8,80,256]{2,1,0:T(8,128)(2,1)S(1)} async-done(((bf16[8,80,256]{2,1,0:T(8,128)(2,1)}), bf16[8,80,256]{2,1,0:T(8,128)(2,1)S(1)}, u32[]{:S(2)}, u32[]{:S(2)}) %all-to-all-start) | async-done | bytes 327712 | tf_op jit(solution)/shard_map/all_to_all | solution.py:412
  140.5 5.1 %shard_map.208 = (bf16[2048,256]{1,0:T(8,128)(2,1)}, bf16[2048,256]{1,0:T(8,128)(2,1)}, bf16[256,2048]{1,0:T(8,128)(2,1)}) custom-call(bf16[64,1024]{1,0:T(8,128)(2,1)S(1)} %shard_map.200.refs_0_, bf16[64,1024]{1,0:T(8,128)(2,1)S(1)} %copy-done.32, bf16[64,1024]{1,0:T(8,128)(2,1)S(1)} %copy-done.30, bf16[64,1024]{1,0:T(8,128)(2,1)S(1)} %copy-done.34, ...), custom_call_target="tpu_custom_call" | custom-call | flops 1610612736 | bytes 8126464 | tf_op jit(solution)/shard_map/pallas_call | solution.py:37
  146.8 2.1 %shard_map.219 = f32[256,512]{1,0:T(8,128)} custom-call(bf16[8,80,256]{2,1,0:T(8,128)(2,1)S(1)} %all-to-all-done.own_ref.got_ref, bf16[8,80,256]{2,1,0:T(8,128)(2,1)S(1)} %collective-permute-done.37.other_ref, bf16[128,512]{1,0:T(8,128)(2,1)S(1)} %get-tuple-element.110.refs_0_, bf16[128,512]{1,0:T(8,128)(2,1)S(1)} %collective-permute-done.38.refs_1_, ...), custom_call_target="tpu_custom_call" | custom-call | flops 268435456 | bytes 2228224 | tf_op jit(solution)/shard_map/pallas_call | solution.py:37
  (219 shorter events, 62.5 us)
Async XLA Ops:
  15.6 23.7 %collective-permute-start.7 = (bf16[192,1024]{1,0:T(8,128)(2,1)S(1)}, bf16[192,1024]{1,0:T(8,128)(2,1)S(1)}, u32[]{:S(2)}, u32[]{:S(2)}) collective-permute-start(bf16[192,1024]{1,0:T(8,128)(2,1)S(1)} %shard_map.201.refs_0_.refs_4_), channel_id=1, source_target_pairs={{0,2},{1,3},{2,0},{3,1},{4,6},{5,7},{6,4},{7,5},{8,10},{9,11},{10,... | collective-permute-start | bytes 1179656 | tf_op jit(solution)/shard_map/ppermute | solution.py:20
  17.3 18.0 %collective-permute-start.10 = (bf16[64,1024]{1,0:T(8,128)(2,1)S(1)}, bf16[64,1024]{1,0:T(8,128)(2,1)S(1)}, u32[]{:S(2)}, u32[]{:S(2)}) collective-permute-start(bf16[64,1024]{1,0:T(8,128)(2,1)S(1)} %get-tuple-element.63), channel_id=1, source_target_pairs={{0,20},{4,16},{8,28},{12,24},{16,4},{20,0},{24,12},{28,8},{1,21},{... | collective-permute-start | bytes 393224 | tf_op jit(solution)/shard_map/ppermute | solution.py:20
  20.9 17.3 %collective-permute-start.9 = (bf16[64,1024]{1,0:T(8,128)(2,1)S(1)}, bf16[64,1024]{1,0:T(8,128)(2,1)S(1)}, u32[]{:S(2)}, u32[]{:S(2)}) collective-permute-start(bf16[64,1024]{1,0:T(8,128)(2,1)S(1)} %get-tuple-element.62), channel_id=1, source_target_pairs={{0,16},{4,20},{8,24},{12,28},{16,0},{20,4},{24,8},{28,12},{1,17},{... | collective-permute-start | bytes 393224 | tf_op jit(solution)/shard_map/ppermute | solution.py:20
  21.2 17.0 %collective-permute-start.14 = (bf16[64,1024]{1,0:T(8,128)(2,1)S(1)}, bf16[64,1024]{1,0:T(8,128)(2,1)S(1)}, u32[]{:S(2)}, u32[]{:S(2)}) collective-permute-start(bf16[64,1024]{1,0:T(8,128)(2,1)S(1)} %get-tuple-element.64), channel_id=1, source_target_pairs={{0,24},{4,28},{8,16},{12,20},{16,8},{20,12},{24,0},{28,4},{1,25},{... | collective-permute-start | bytes 393224 | tf_op jit(solution)/shard_map/ppermute | solution.py:20
  24.8 13.9 %collective-permute-start.15 = (bf16[64,1024]{1,0:T(8,128)(2,1)S(1)}, bf16[64,1024]{1,0:T(8,128)(2,1)S(1)}, u32[]{:S(2)}, u32[]{:S(2)}) collective-permute-start(bf16[64,1024]{1,0:T(8,128)(2,1)S(1)} %get-tuple-element.65), channel_id=1, source_target_pairs={{0,28},{4,24},{8,20},{12,16},{16,12},{20,8},{24,4},{28,0},{1,29},{... | collective-permute-start | bytes 393224 | tf_op jit(solution)/shard_map/ppermute | solution.py:20
  38.2 14.5 %collective-permute-start.6 = (bf16[192,1024]{1,0:T(8,128)(2,1)S(1)}, bf16[192,1024]{1,0:T(8,128)(2,1)S(1)}, u32[]{:S(2)}, u32[]{:S(2)}) collective-permute-start(bf16[192,1024]{1,0:T(8,128)(2,1)S(1)} %shard_map.201.refs_0_.refs_4_), channel_id=1, source_target_pairs={{0,1},{1,0},{2,3},{3,2},{4,5},{5,4},{6,7},{7,6},{8,9},{9,8},{10,11... | collective-permute-start | bytes 1179656 | tf_op jit(solution)/shard_map/ppermute | solution.py:20
  38.7 9.2 %collective-permute-start.12 = (bf16[128,1024]{1,0:T(8,128)(2,1)S(1)}, bf16[128,1024]{1,0:T(8,128)(2,1)S(1)}, u32[]{:S(2)}, u32[]{:S(2)}) collective-permute-start(bf16[128,1024]{1,0:T(8,128)(2,1)S(1)} %shard_map.202.refs_0_.refs_8_), channel_id=1, source_target_pairs={{0,2},{1,3},{2,0},{3,1},{4,6},{5,7},{6,4},{7,5},{8,10},{9,11},{10,... | collective-permute-start | bytes 786440 | tf_op jit(solution)/shard_map/ppermute | solution.py:20
  39.3 17.6 %collective-permute-start.8 = (bf16[192,1024]{1,0:T(8,128)(2,1)S(1)}, bf16[192,1024]{1,0:T(8,128)(2,1)S(1)}, u32[]{:S(2)}, u32[]{:S(2)}) collective-permute-start(bf16[192,1024]{1,0:T(8,128)(2,1)S(1)} %collective-permute-done.7.refs_2_.refs_6_), channel_id=1, source_target_pairs={{0,1},{1,0},{2,3},{3,2},{4,5},{5,4},{6,7},{7,6},{8,9},{9,8},{10,11... | collective-permute-start | bytes 1179656 | tf_op jit(solution)/shard_map/ppermute | solution.py:20
  40.3 12.3 %collective-permute-start.17 = (bf16[128,1024]{1,0:T(8,128)(2,1)S(1)}, bf16[128,1024]{1,0:T(8,128)(2,1)S(1)}, u32[]{:S(2)}, u32[]{:S(2)}) collective-permute-start(bf16[128,1024]{1,0:T(8,128)(2,1)S(1)} %shard_map.203.refs_0_.refs_12_), channel_id=1, source_target_pairs={{0,2},{1,3},{2,0},{3,1},{4,6},{5,7},{6,4},{7,5},{8,10},{9,11},{10,... | collective-permute-start | bytes 786440 | tf_op jit(solution)/shard_map/ppermute | solution.py:20
  42.3 18.1 %collective-permute-start.11 = (bf16[128,1024]{1,0:T(8,128)(2,1)S(1)}, bf16[128,1024]{1,0:T(8,128)(2,1)S(1)}, u32[]{:S(2)}, u32[]{:S(2)}) collective-permute-start(bf16[128,1024]{1,0:T(8,128)(2,1)S(1)} %shard_map.202.refs_0_.refs_8_), channel_id=1, source_target_pairs={{0,1},{1,0},{2,3},{3,2},{4,5},{5,4},{6,7},{7,6},{8,9},{9,8},{10,11... | collective-permute-start | bytes 786440 | tf_op jit(solution)/shard_map/ppermute | solution.py:20
  48.0 12.4 %collective-permute-start.13 = (bf16[128,1024]{1,0:T(8,128)(2,1)S(1)}, bf16[128,1024]{1,0:T(8,128)(2,1)S(1)}, u32[]{:S(2)}, u32[]{:S(2)}) collective-permute-start(bf16[128,1024]{1,0:T(8,128)(2,1)S(1)} %collective-permute-done.12.refs_2_.refs_10_), channel_id=1, source_target_pairs={{0,1},{1,0},{2,3},{3,2},{4,5},{5,4},{6,7},{7,6},{8,9},{9,8},{10,11... | collective-permute-start | bytes 786440 | tf_op jit(solution)/shard_map/ppermute | solution.py:20
  52.6 9.8 %collective-permute-start.16 = (bf16[128,1024]{1,0:T(8,128)(2,1)S(1)}, bf16[128,1024]{1,0:T(8,128)(2,1)S(1)}, u32[]{:S(2)}, u32[]{:S(2)}) collective-permute-start(bf16[128,1024]{1,0:T(8,128)(2,1)S(1)} %shard_map.203.refs_0_.refs_12_), channel_id=1, source_target_pairs={{0,1},{1,0},{2,3},{3,2},{4,5},{5,4},{6,7},{7,6},{8,9},{9,8},{10,11... | collective-permute-start | bytes 786440 | tf_op jit(solution)/shard_map/ppermute | solution.py:20
  52.7 9.8 %collective-permute-start.18 = (bf16[128,1024]{1,0:T(8,128)(2,1)S(1)}, bf16[128,1024]{1,0:T(8,128)(2,1)S(1)}, u32[]{:S(2)}, u32[]{:S(2)}) collective-permute-start(bf16[128,1024]{1,0:T(8,128)(2,1)S(1)} %collective-permute-done.17.refs_2_.refs_14_), channel_id=1, source_target_pairs={{0,1},{1,0},{2,3},{3,2},{4,5},{5,4},{6,7},{7,6},{8,9},{9,8},{10,11... | collective-permute-start | bytes 786440 | tf_op jit(solution)/shard_map/ppermute | solution.py:20
  65.9 11.7 %collective-permute-start.21 = (bf16[192,1024]{1,0:T(8,128)(2,1)S(1)}, bf16[192,1024]{1,0:T(8,128)(2,1)S(1)}, u32[]{:S(2)}, u32[]{:S(2)}) collective-permute-start(bf16[192,1024]{1,0:T(8,128)(2,1)S(1)} %get-tuple-element.87), channel_id=1, source_target_pairs={{0,1},{1,0},{2,3},{3,2},{4,5},{5,4},{6,7},{7,6},{8,9},{9,8},{10,11... | collective-permute-start | bytes 1179656 | tf_op jit(solution)/shard_map/ppermute | solution.py:20
  68.5 20.1 %collective-permute-start.20 = (bf16[64,512]{1,0:T(8,128)(2,1)S(1)}, bf16[64,512]{1,0:T(8,128)(2,1)S(1)}, u32[]{:S(2)}, u32[]{:S(2)}) collective-permute-start(bf16[64,512]{1,0:T(8,128)(2,1)S(1)} %get-tuple-element.85), channel_id=1, source_target_pairs={{0,2},{1,3},{2,0},{3,1},{4,6},{5,7},{6,4},{7,5},{8,10},{9,11},{10,... | collective-permute-start | bytes 196616 | tf_op jit(solution)/shard_map/ppermute | solution.py:20
  69.6 8.6 %collective-permute-start.27 = (bf16[128,512]{1,0:T(8,128)(2,1)S(1)}, bf16[128,512]{1,0:T(8,128)(2,1)S(1)}, u32[]{:S(2)}, u32[]{:S(2)}) collective-permute-start(bf16[128,512]{1,0:T(8,128)(2,1)S(1)} %get-tuple-element.96), channel_id=1, source_target_pairs={{0,2},{1,3},{2,0},{3,1},{4,6},{5,7},{6,4},{7,5},{8,10},{9,11},{10,... | collective-permute-start | bytes 393224 | tf_op jit(solution)/shard_map/ppermute | solution.py:20
  73.8 16.6 %collective-permute-start.32 = (bf16[64,512]{1,0:T(8,128)(2,1)S(1)}, bf16[64,512]{1,0:T(8,128)(2,1)S(1)}, u32[]{:S(2)}, u32[]{:S(2)}) collective-permute-start(bf16[64,512]{1,0:T(8,128)(2,1)S(1)} %get-tuple-element.103), channel_id=1, source_target_pairs={{0,24},{4,28},{8,16},{12,20},{16,8},{20,12},{24,0},{28,4},{1,25},{... | collective-permute-start | bytes 196616 | tf_op jit(solution)/shard_map/ppermute | solution.py:20
  76.0 14.4 %collective-permute-start.33 = (bf16[64,512]{1,0:T(8,128)(2,1)S(1)}, bf16[64,512]{1,0:T(8,128)(2,1)S(1)}, u32[]{:S(2)}, u32[]{:S(2)}) collective-permute-start(bf16[64,512]{1,0:T(8,128)(2,1)S(1)} %get-tuple-element.104), channel_id=1, source_target_pairs={{0,28},{4,24},{8,20},{12,16},{16,12},{20,8},{24,4},{28,0},{1,29},{... | collective-permute-start | bytes 196616 | tf_op jit(solution)/shard_map/ppermute | solution.py:20
  78.3 14.0 %collective-permute-start.28 = (bf16[64,512]{1,0:T(8,128)(2,1)S(1)}, bf16[64,512]{1,0:T(8,128)(2,1)S(1)}, u32[]{:S(2)}, u32[]{:S(2)}) collective-permute-start(bf16[64,512]{1,0:T(8,128)(2,1)S(1)} %get-tuple-element.97), channel_id=1, source_target_pairs={{0,16},{4,20},{8,24},{12,28},{16,0},{20,4},{24,8},{28,12},{1,17},{... | collective-permute-start | bytes 196616 | tf_op jit(solution)/shard_map/ppermute | solution.py:20
  83.8 8.5 %collective-permute-start.29 = (bf16[64,512]{1,0:T(8,128)(2,1)S(1)}, bf16[64,512]{1,0:T(8,128)(2,1)S(1)}, u32[]{:S(2)}, u32[]{:S(2)}) collective-permute-start(bf16[64,512]{1,0:T(8,128)(2,1)S(1)} %get-tuple-element.98), channel_id=1, source_target_pairs={{0,20},{4,16},{8,28},{12,24},{16,4},{20,0},{24,12},{28,8},{1,21},{... | collective-permute-start | bytes 196616 | tf_op jit(solution)/shard_map/ppermute | solution.py:20
  103.8 8.0 %collective-permute-start.39 = (bf16[256,512]{1,0:T(8,128)(2,1)}, bf16[256,512]{1,0:T(8,128)(2,1)S(1)}, u32[]{:S(2)}, u32[]{:S(2)}) collective-permute-start(bf16[256,512]{1,0:T(8,128)(2,1)} %pad_maximum_fusion.1), channel_id=1, source_target_pairs={{0,8},{4,12},{8,0},{12,4},{16,24},{20,28},{24,16},{28,20},{1,9},{5... | collective-permute-start | bytes 786440 | tf_op jit(solution)/shard_map/ppermute | solution.py:20
  108.2 12.7 %all-to-all-start = ((bf16[8,80,256]{2,1,0:T(8,128)(2,1)}), bf16[8,80,256]{2,1,0:T(8,128)(2,1)S(1)}, u32[]{:S(2)}, u32[]{:S(2)}) async-start(bf16[8,80,256]{2,1,0:T(8,128)(2,1)} %get-tuple-element.106), calls=%async_computation | async-start | bytes 655360 | tf_op jit(solution)/shard_map/all_to_all | solution.py:412
  112.7 34.1 %collective-permute-start.40 = (bf16[512,512]{1,0:T(8,128)(2,1)}, bf16[512,512]{1,0:T(8,128)(2,1)S(1)}, u32[]{:S(2)}, u32[]{:S(2)}) collective-permute-start(bf16[512,512]{1,0:T(8,128)(2,1)} %pad_maximum_fusion), channel_id=1, source_target_pairs={{0,4},{4,0},{8,12},{12,8},{16,20},{20,16},{24,28},{28,24},{1,5},{5... | collective-permute-start | bytes 1572872 | tf_op jit(solution)/shard_map/ppermute | solution.py:20
  120.9 25.9 %collective-permute-start.37 = (bf16[8,80,256]{2,1,0:T(8,128)(2,1)S(1)}, bf16[8,80,256]{2,1,0:T(8,128)(2,1)S(1)}, u32[]{:S(2)}, u32[]{:S(2)}) collective-permute-start(bf16[8,80,256]{2,1,0:T(8,128)(2,1)S(1)} %all-to-all-done.own_ref.got_ref), channel_id=1, source_target_pairs={{0,1},{1,0},{2,3},{3,2},{4,5},{5,4},{6,7},{7,6},{8,9},{9,8},{10,11... | collective-permute-start | bytes 983048 | tf_op jit(solution)/shard_map/ppermute | solution.py:20
  (84 other events, 582.8 us)
where the time goes:
time: 150 us; the launch traced here: 149 us
  waiting for transfers between devices  49.3 us (33%)
  starting transfers between devices  48.6 us (32%)
  local copies, waits for them, and re-layouts  28 us (19%)
  Pallas kernels  19.5 us (13%)
  other arithmetic  2.27 us (2%)
    ppermute x41, starting transfers between devices, hop(): return lax.ppermute(value, axis, [(i, i ^ bit) for i in range(count)])  45 us
    ppermute x41, waiting for transfers between devices, hop(): return lax.ppermute(value, axis, [(i, i ^ bit) for i in range(count)])  42.8 us
    unnamed x132, local copies, waits for them, and re-layouts  28 us
    pallas_call x22, Pallas kernels, call(): pl.pallas_call(kernel, out_shape=list(outs), in_specs=specs, out_specs=[V...  19.5 us
    all_to_all x1, waiting for transfers between devices, body(): own = lax.all_to_all(slices, 'sp', split_axis=0, concat_axis=0, tiled=True)  6.5 us
    all_to_all x1, starting transfers between devices, body(): own = lax.all_to_all(slices, 'sp', split_axis=0, concat_axis=0, tiled=True)  3.61 us
  transfers between devices with their start and end apart: 42, of which 18 were waited for; matrix products, arithmetic and copies ran while one was open for 2% of the time, Pallas kernels for 10%

commit v1 on v0

--- a/solution.py
+++ b/solution.py
@@ -87,9 +87,17 @@
         block[:, feat:] = cots[k * cap : (k + 1) * cap]
 
 
-def expert_kernel(m, *refs):
+def expert_kernel(m, groups, *refs):
     me = lax.axis_index("tp")
-    parts, (wg_ref, wu_ref, wd_ref) = refs[:m], refs[m : m + 3]
+    parts, (wg_ref, wu_ref, wd_ref) = refs[:m], refs[groups * m : groups * m + 3]
+    if groups > 1:
+        parts, refs = refs[-m:], refs[:-m]
+        for q in range(m):
+            at = 0
+            for g in range(groups):
+                piece = refs[g * m + q]
+                parts[q][at : at + piece.shape[0], :] = piece[...]
+                at += piece.shape[0]
     dg_ref, du_ref, act_ref, keep_ref, send_ref = refs[-5:]
     feat = parts[0].shape[1] // 2
 
@@ -135,9 +143,10 @@
 
 
 def join_kernel(*refs):
-    rows = refs[0].shape[0]
-    for i, ref in enumerate(refs[:-1]):
-        refs[-1][i * rows : (i + 1) * rows, :] = ref[...]
+    at = 0
+    for ref in refs[:-1]:
+        refs[-1][at : at + ref.shape[0], :] = ref[...]
+        at += ref.shape[0]
 
 
 def halve_kernel(feat, keep_ref, got_ref, stay_ref, go_ref):
@@ -156,11 +165,27 @@
         out[...] = total[k * cap : (k + 1) * cap]
 
 
-def combine_kernel(n, cap, d_ref, cot_ref, *refs):
-    blocks, out_ref, held = refs[:n], refs[-2], refs[-1]
-    for k in range(n):
-        held[k * cap : (k + 1) * cap, :] = blocks[k][...]
-    out_ref[...] = (dot_tn(d_ref[...], held[...]) + cot_ref[...].astype(F32)).astype(BF)
+def near_kernel(cap, d_ref, cot_ref, *refs):
+    blocks, (stay_ref, go_ref, held) = refs[:-3], refs[-3:]
+    feat, rows = cot_ref.shape[1], held.shape[0]
+    for k, block in enumerate(blocks):
+        held[k * cap : (k + 1) * cap, :] = block[...]
+    total = dot_tn(d_ref[:rows, :], held[...])
+    for i in range(held.shape[1] // feat):
+        part = total[:, i * feat : (i + 1) * feat]
+        if i == 0:
+            part = part + cot_ref[...].astype(F32)
+        at = slice((i >> 1) * feat, ((i >> 1) + 1) * feat)
+        target = go_ref if i & 1 else stay_ref
+        target[:, at] = part.astype(target.dtype)
+
+
+def combine_kernel(cap, d_ref, near_ref, got_ref, *refs):
+    blocks, (out_ref, held) = refs[:-2], refs[-2:]
+    for k, block in enumerate(blocks):
+        held[k * cap : (k + 1) * cap, :] = block[...]
+    total = dot_tn(d_ref[d_ref.shape[0] - held.shape[0] :, :], held[...])
+    out_ref[...] = (total + near_ref[...] + got_ref[...].astype(F32)).astype(BF)
 
 
 def recur_kernel(n, m, *refs):
@@ -234,18 +259,20 @@
 
 
 def out_proj_kernel(n, tok, orders, own_ref, other_ref, *refs):
-    pieces, out_ref, held = refs[: len(orders)], refs[-2], refs[-1]
+    pieces, (out_ref, held, grad) = refs[: len(orders)], refs[-3:]
     half = tok // 2
     me, side = lax.axis_index("sp"), lax.axis_index("tp") & 1
     for piece, order in zip(pieces, orders):
         for i, k in enumerate(order):
             held[me ^ k] = piece[i * tok : (i + 1) * tok]
-    total = 0.0
     for s in range(n):
         for part, bit in ((own_ref, 0), (other_ref, 1)):
             at = pl.ds(pl.multiple_of((side ^ bit) * half, half), half)
-            total += dot_tn(part[s, :half, :], held[s, at, :])
-    out_ref[...] = total
+            grad[s, at, :] = part[s, :half, :]
+    flat = grad.shape[0] * grad.shape[1]
+    out_ref[...] = dot_tn(
+        grad[...].reshape(flat, grad.shape[2]), held[...].reshape(flat, held.shape[2])
+    )
 
 
 def body(
@@ -287,9 +314,10 @@
             pltpu.VMEM((tok, feat), BF),
             pltpu.SemaphoreType.DMA((4,)),
         ],
+        limit=60,
     )
     pick, first, sent = sent[0], sent[1], sent[2:]
-    edges = [0, 1, n // 2, 3 * n // 4, n]
+    edges = [0, n // 4, n // 2, 3 * n // 4, n]
     chunks = [range(a, b) for a, b in zip(edges, edges[1:])]
     got = [sent[0]] + [hop(sent[k], "sp", k) for k in range(1, n)]
 
@@ -313,37 +341,56 @@
     c3 = norm_factor * input_f
     c2 = c3 * conv_f * (1.0 - input_f)
 
-    parts, grads, back = [], [], [None] * n
-    before = []
-    for chunk in chunks:
+    groups, parts, grads, back, before = [], [], [], [], []
+    half_width = m * feat // 2
+    for h, chunk in enumerate(chunks):
         rows = len(chunk) * cap
-        joined = call(
-            join_kernel,
-            [struct((rows, 2 * feat), BF)],
-            [got[k] for k in chunk],
-            [VM] * len(chunk),
-            rows * feat,
-        )
+        joined = [got[k] for k in chunk]
+        if len(chunk) > 1:
+            joined = call(
+                join_kernel, [struct((rows, 2 * feat), BF)], joined, [VM] * len(chunk), rows * feat
+            )
         here = {0: joined[0]}
         if chunk is chunks[-1]:
-            pieces, orders = [mixed, hop(mixed, "sp", n // 2)], [[0], [n // 2]]
+            pieces = [mixed, hop(mixed, "sp", n // 2)]
         bit = m // 2
         while bit:
             for q in sorted(here):
                 here[q | bit] = hop(here[q], "tp", bit)
             bit //= 2
-        piece = [here[q] for q in range(m)]
-        d_gate, d_up, active, keep, give = call(
-            functools.partial(expert_kernel, m),
-            [struct((rows, hidden), BF)] * 3 + [struct((rows, m * feat // 2), BF)] * 2,
-            piece + [wg, wu, wd] + before,
-            [VM] * (m + 3) + [ANY] * len(before),
+        groups.append([here[q] for q in range(m)])
+        if h == 0:
+            continue
+        merged = []
+        if h == 1:
+            rows += len(chunks[0]) * cap
+            merged = [struct((rows, 2 * feat), BF)] * m
+        given = [a for group in groups for a in group]
+        made = call(
+            functools.partial(expert_kernel, m, len(groups)),
+            [struct((rows, hidden), BF)] * 3 + [struct((rows, half_width), BF)] * 2 + merged,
+            given + [wg, wu, wd] + before,
+            [VM] * (len(given) + 3) + [ANY] * len(before),
             10 * rows * m * feat * hidden,
             limit=16,
         )
+        d_gate, d_up, active, keep, give = made[:5]
         before = [d_up]
-        parts.append(piece)
+        parts.append(made[5:] if merged else groups[0])
+        groups = []
         grads.append([d_gate, d_up, active])
+        if h == 1:
+            blocks = call(
+                functools.partial(finish_kernel, cap),
+                [struct((cap, half_width), BF)] * (n // 2),
+                [keep, hop(give, "tp", 1)],
+                [VM, VM],
+                rows * half_width,
+            )
+            near = [blocks[0]]
+            for k in range(1, n // 2):
+                near.append(hop(blocks[k], "sp", k))
+            continue
         bit = 1
         while 2 * bit < m:
             keep, give = call(
@@ -361,34 +408,56 @@
             [VM, VM],
             rows * feat,
         )
-        for k, block in zip(chunk, blocks):
-            back[k] = hop(block, "sp", k) if k else block
-
-    bit = n // 4
+        back += [hop(block, "sp", k) for k, block in zip(chunk, blocks)]
+
+    stacked = call(
+        join_kernel, [struct((2 * tok, channels), BF)], pieces, [VM] * 2, tok * channels
+    )[0]
+    sources, bit = [(stacked, [0, n // 2])], n // 4
     while bit:
-        stacked = jnp.concatenate(pieces, axis=0)
-        order = [k for group in orders for k in group]
-        pieces.append(hop(stacked, "sp", bit))
-        orders.append([k | bit for k in order])
+        for source, order in list(sources):
+            moved = hop(source, "sp", bit)
+            sources.append((moved, [k | bit for k in order]))
         bit //= 2
+    pieces = [source for source, _ in sources]
+    orders = [order for _, order in sources]
 
     grad_gate, grad_up, grad_down = call(
-        functools.partial(weight_kernel, m, len(chunks)),
+        functools.partial(weight_kernel, m, len(parts)),
         [struct(wg.shape, BF), struct(wu.shape, BF), struct(wd.shape, BF)],
         [a for piece in parts for a in piece] + [a for g in grads for a in g],
-        [VM] * (len(chunks) * (m + 3)),
+        [VM] * (len(parts) * (m + 3)),
         6 * slots * m * feat * hidden,
         limit=24,
     )
 
+    near_rows = slots // 2
+    stay, go = call(
+        functools.partial(near_kernel, cap),
+        [struct((tok, half_width // 2), t) for t in (F32, BF)],
+        [pick, cotangent, *near],
+        [VM] * (n // 2 + 2),
+        2 * near_rows * tok * half_width,
+        scratch=[pltpu.VMEM((near_rows, half_width), BF)],
+    )
+    bit = 2
+    while 2 * bit < m:
+        stay, go = call(
+            functools.partial(halve_kernel, feat),
+            [struct((tok, stay.shape[1] // 2), t) for t in (F32, BF)],
+            [stay, hop(go, "tp", bit)],
+            [VM, VM],
+            tok * m * feat,
+        )
+        bit *= 2
     out_grad = {
         0: call(
-            functools.partial(combine_kernel, n, cap),
+            functools.partial(combine_kernel, cap),
             [struct((tok, feat), BF)],
-            [pick, cotangent, *back],
-            [VM] * (n + 2),
-            2 * slots * tok * feat,
-            scratch=[pltpu.VMEM((slots, feat), BF)],
+            [pick, stay, hop(go, "tp", bit), *back],
+            [VM] * (len(back) + 3),
+            2 * near_rows * tok * feat,
+            scratch=[pltpu.VMEM((slots - near_rows, feat), BF)],
         )[0]
     }
     bit = m // 2
@@ -424,7 +493,7 @@
         [own, other, *pieces],
         [VM] * (2 + len(pieces)),
         2 * n * tok * width * channels,
-        scratch=[pltpu.VMEM((n, tok, channels), BF)],
+        scratch=[pltpu.VMEM((n, tok, channels), BF), pltpu.VMEM((n, tok, width), BF)],
         limit=32 if n > 8 else 8,
     )[0]
     return (

time: 150 us -> 143 us (0.953)
  local copies, waits for them, and re-layouts: 28 us -> 16.8 us
  waiting for transfers between devices: 49.3 us -> 53.8 us
  starting transfers between devices: 48.6 us -> 51.3 us
  other arithmetic: 2.27 us -> 0.72 us
    unnamed x132 -> x88, local copies, waits for them, and re-layouts: 28 us -> 16.8 us
    ppermute x41 -> x40, waiting for transfers between devices: 42.8 us -> 53.8 us  [hop(): return lax.ppermute(value, axis, [(i, i ^ bit) for i in range(count)])]
    all_to_all x1, waiting for transfers between devices: 6.5 us -> 0.01 us  [body(): own = lax.all_to_all(slices, 'sp', split_axis=0, concat_axis=0, tiled=True)]
    ppermute x41 -> x40, starting transfers between devices: 45 us -> 47.5 us  [hop(): return lax.ppermute(value, axis, [(i, i ^ bit) for i in range(count)])]
    concatenate x2 -> x0, other arithmetic: 1.55 us -> none  [body(): stacked = jnp.concatenate(pieces, axis=0)]
    pallas_call x22 -> x20, Pallas kernels: 19.5 us -> 18.8 us  [call(): pl.pallas_call(kernel, out_shape=list(outs), in_specs=specs, out_specs=[V...]
  transfers between devices with their start and end apart: 42 -> 41, of which waited for: 18 -> 12; matrix products, arithmetic and copies ran while one was open for 2% -> 1% of each run, Pallas kernels for 10% -> 8%
where the time goes in v1:
time: 143 us
  waiting for transfers between devices  53.8 us (38%)
  starting transfers between devices  51.3 us (36%)
  Pallas kernels  18.8 us (13%)
  local copies, waits for them, and re-layouts  16.8 us (12%)
    ppermute x40, waiting for transfers between devices, hop(): return lax.ppermute(value, axis, [(i, i ^ bit) for i in range(count)])  53.8 us
    ppermute x40, starting transfers between devices, hop(): return lax.ppermute(value, axis, [(i, i ^ bit) for i in range(count)])  47.5 us
    pallas_call x20, Pallas kernels, call(): pl.pallas_call(kernel, out_shape=list(outs), in_specs=specs, out_specs=[V...  18.8 us
    unnamed x88, local copies, waits for them, and re-layouts  16.8 us
    all_to_all x1, starting transfers between devices, body(): own = lax.all_to_all(slices, 'sp', split_axis=0, concat_axis=0, tiled=True)  3.86 us
  transfers between devices with their start and end apart: 41, of which 12 were waited for; matrix products, arithmetic and copies ran while one was open for 1% of the time, Pallas kernels for 8%

profile of v1, /device:TPU:0, one launch (start us, length us, event | category | flops | bytes accessed | tf_op | source)
XLA Modules:
  0.0 142.6 jit_solution(12308470574343484328)
XLA Ops:
  0.7 2.7 %shard_map.199 = (bf16[512,128]{1,0:T(8,128)(2,1)}, f32[128,128]{1,0:T(8,128)}, bf16[64,1024]{1,0:T(8,128)(2,1)}, bf16[64,1024]{1,0:T(8,128)(2,1)}, bf16[64,1024...) custom-call(s32[2,128]{1,0:T(2,128)} %bitcast.17, ...), custom_call_target="tpu_custom_call" | custom-call | flops 134217728 | bytes 1509376 | tf_op jit(solution)/shard_map/pallas_call | solution.py:37
  3.4 3.1 %collective-permute-start.4 = (bf16[64,1024]{1,0:T(8,128)(2,1)}, bf16[64,1024]{1,0:T(8,128)(2,1)S(1)}, u32[]{:S(2)}, u32[]{:S(2)}) collective-permute-start(bf16[64,1024]{1,0:T(8,128)(2,1)} %get-tuple-element.58), channel_id=1, source_target_pairs={{0,8},{4,12},{8,0},{12,4},{16,24},{20,28},{24,16},{28,20},{1,9},{5... | collective-permute-start | bytes 393224 | tf_op jit(solution)/shard_map/ppermute | solution.py:20
  8.1 3.9 %collective-permute-start.10 = (bf16[64,1024]{1,0:T(8,128)(2,1)}, bf16[64,1024]{1,0:T(8,128)(2,1)S(1)}, u32[]{:S(2)}, u32[]{:S(2)}) collective-permute-start(bf16[64,1024]{1,0:T(8,128)(2,1)} %get-tuple-element.65), channel_id=1, source_target_pairs={{0,20},{4,16},{8,28},{12,24},{16,4},{20,0},{24,12},{28,8},{1,21},{... | collective-permute-start | bytes 393224 | tf_op jit(solution)/shard_map/ppermute | solution.py:20
  12.0 5.0 %collective-permute-done.5.refs_1_ = bf16[64,1024]{1,0:T(8,128)(2,1)S(1)} collective-permute-done((bf16[64,1024]{1,0:T(8,128)(2,1)}, bf16[64,1024]{1,0:T(8,128)(2,1)S(1)}, u32[]{:S(2)}, u32[]{:S(2)}) %collective-permute-start.5) | collective-permute-done | bytes 131104 | tf_op jit(solution)/shard_map/ppermute | solution.py:20
  20.9 2.6 %collective-permute-start.9 = (bf16[64,1024]{1,0:T(8,128)(2,1)}, bf16[64,1024]{1,0:T(8,128)(2,1)S(1)}, u32[]{:S(2)}, u32[]{:S(2)}) collective-permute-start(bf16[64,1024]{1,0:T(8,128)(2,1)} %get-tuple-element.64), channel_id=1, source_target_pairs={{0,16},{4,20},{8,24},{12,28},{16,0},{20,4},{24,8},{28,12},{1,17},{... | collective-permute-start | bytes 393224 | tf_op jit(solution)/shard_map/ppermute | solution.py:20
  24.9 2.4 %collective-permute-start.15 = (bf16[64,1024]{1,0:T(8,128)(2,1)}, bf16[64,1024]{1,0:T(8,128)(2,1)S(1)}, u32[]{:S(2)}, u32[]{:S(2)}) collective-permute-start(bf16[64,1024]{1,0:T(8,128)(2,1)} %get-tuple-element.67), channel_id=1, source_target_pairs={{0,28},{4,24},{8,20},{12,16},{16,12},{20,8},{24,4},{28,0},{1,29},{... | collective-permute-start | bytes 393224 | tf_op jit(solution)/shard_map/ppermute | solution.py:20
  27.3 8.1 %collective-permute-done.9.refs_0_ = bf16[64,1024]{1,0:T(8,128)(2,1)S(1)} collective-permute-done((bf16[64,1024]{1,0:T(8,128)(2,1)}, bf16[64,1024]{1,0:T(8,128)(2,1)S(1)}, u32[]{:S(2)}, u32[]{:S(2)}) %collective-permute-start.9) | collective-permute-done | bytes 131104 | tf_op jit(solution)/shard_map/ppermute | solution.py:20
  38.7 6.5 %collective-permute-done.12.refs_2_.refs_6_ = bf16[128,1024]{1,0:T(8,128)(2,1)S(1)} collective-permute-done((bf16[128,1024]{1,0:T(8,128)(2,1)S(1)}, bf16[128,1024]{1,0:T(8,128)(2,1)S(1)}, u32[]{:S(2)}, u32[]{:S(2)}) %collective-permute-start.12) | collective-permute-done | bytes 262176 | tf_op jit(solution)/shard_map/ppermute | solution.py:20
  46.5 2.2 %shard_map.202 = (bf16[256,256]{1,0:T(8,128)(2,1)S(1)}, bf16[256,256]{1,0:T(8,128)(2,1)S(1)}, bf16[256,256]{1,0:T(8,128)(2,1)S(1)}, bf16[256,1024]{1,0:T(8,128)(...) custom-call(bf16[128,1024]{1,0:T(8,128)(2,1)S(1)} %shard_map.200.ref, ...), custom_call_target="tpu_custom_call" | custom-call | flops 1342177280 | bytes 8781824 | tf_op jit(solution)/shard_map/pallas_call | solution.py:37
  50.5 1.9 %shard_map.205 = (bf16[128,256]{1,0:T(8,128)(2,1)S(1)}, bf16[128,256]{1,0:T(8,128)(2,1)S(1)}, bf16[128,256]{1,0:T(8,128)(2,1)S(1)}, bf16[128,1024]{1,0:T(8,128)(2,1)S(1)}, bf16[128,1024]{1,0:T(8,128)(2,1)S(1)}) custom-call(bf16[128,1024]{1,0:T(8,128)(2,1)S(1)} %shard_map.203.refs_0_.refs_4_, bf16[128,1024]{1,0:T(8,128)(2,1)S(1)} %collective-permute-done.11.refs_1_.refs_5_, ...), custom_call_target="tpu_custom_call" | custom-call | flops 671088640 | bytes 5046272 | tf_op jit(solution)/shard_map/pallas_call | solution.py:37
  53.2 1.9 %shard_map.206 = (bf16[128,256]{1,0:T(8,128)(2,1)S(1)}, bf16[128,256]{1,0:T(8,128)(2,1)S(1)}, bf16[128,256]{1,0:T(8,128)(2,1)S(1)}, bf16[128,1024]{1,0:T(8,128)(2,1)S(1)}, bf16[128,1024]{1,0:T(8,128)(2,1)S(1)}) custom-call(bf16[128,1024]{1,0:T(8,128)(2,1)S(1)} %shard_map.204.refs_0_.refs_8_, bf16[128,1024]{1,0:T(8,128)(2,1)S(1)} %collective-permute-done.16.refs_1_.refs_9_, ...), custom_call_target="tpu_custom_call" | custom-call | flops 671088640 | bytes 4980736 | tf_op jit(solution)/shard_map/pallas_call | solution.py:37
  57.1 5.9 %collective-permute-start.21 = (bf16[64,1024]{1,0:T(8,128)(2,1)S(1)}, bf16[64,1024]{1,0:T(8,128)(2,1)S(1)}, u32[]{:S(2)}, u32[]{:S(2)}) collective-permute-start(bf16[64,1024]{1,0:T(8,128)(2,1)S(1)} %get-tuple-element.85), channel_id=1, source_target_pairs={{0,8},{4,12},{8,0},{12,4},{16,24},{20,28},{24,16},{28,20},{1,9},{5... | collective-permute-start | bytes 393224 | tf_op jit(solution)/shard_map/ppermute | solution.py:20
  65.3 2.1 %collective-permute-done.21.refs_2_ = bf16[64,1024]{1,0:T(8,128)(2,1)S(1)} collective-permute-done((bf16[64,1024]{1,0:T(8,128)(2,1)S(1)}, bf16[64,1024]{1,0:T(8,128)(2,1)S(1)}, u32[]{:S(2)}, u32[]{:S(2)}) %collective-permute-start.21) | collective-permute-done | bytes 131104 | tf_op jit(solution)/shard_map/ppermute | solution.py:20
  70.0 2.9 %collective-permute-start.30 = (bf16[64,512]{1,0:T(8,128)(2,1)S(1)}, bf16[64,512]{1,0:T(8,128)(2,1)S(1)}, u32[]{:S(2)}, u32[]{:S(2)}) collective-permute-start(bf16[64,512]{1,0:T(8,128)(2,1)S(1)} %get-tuple-element.99), channel_id=1, source_target_pairs={{0,24},{4,28},{8,16},{12,20},{16,8},{20,12},{24,0},{28,4},{1,25},{... | collective-permute-start | bytes 196616 | tf_op jit(solution)/shard_map/ppermute | solution.py:20
  72.9 2.1 %collective-permute-start.31 = (bf16[64,512]{1,0:T(8,128)(2,1)S(1)}, bf16[64,512]{1,0:T(8,128)(2,1)S(1)}, u32[]{:S(2)}, u32[]{:S(2)}) collective-permute-start(bf16[64,512]{1,0:T(8,128)(2,1)S(1)} %get-tuple-element.100), channel_id=1, source_target_pairs={{0,28},{4,24},{8,20},{12,16},{16,12},{20,8},{24,4},{28,0},{1,29},{... | collective-permute-start | bytes 196616 | tf_op jit(solution)/shard_map/ppermute | solution.py:20
  77.8 2.2 %collective-permute-done.31.refs_3_ = bf16[64,512]{1,0:T(8,128)(2,1)S(1)} collective-permute-done((bf16[64,512]{1,0:T(8,128)(2,1)S(1)}, bf16[64,512]{1,0:T(8,128)(2,1)S(1)}, u32[]{:S(2)}, u32[]{:S(2)}) %collective-permute-start.31) | collective-permute-done | bytes 65568 | tf_op jit(solution)/shard_map/ppermute | solution.py:20
  80.0 4.0 %collective-permute-done.26.refs_0_ = bf16[64,512]{1,0:T(8,128)(2,1)S(1)} collective-permute-done((bf16[64,512]{1,0:T(8,128)(2,1)S(1)}, bf16[64,512]{1,0:T(8,128)(2,1)S(1)}, u32[]{:S(2)}, u32[]{:S(2)}) %collective-permute-start.26) | collective-permute-done | bytes 65568 | tf_op jit(solution)/shard_map/ppermute | solution.py:20
  87.2 3.3 %collective-permute-done.33.refs_2_ = bf16[128,512]{1,0:T(8,128)(2,1)S(1)} collective-permute-done((bf16[128,512]{1,0:T(8,128)(2,1)S(1)}, bf16[128,512]{1,0:T(8,128)(2,1)S(1)}, u32[]{:S(2)}, u32[]{:S(2)}) %collective-permute-start.33) | collective-permute-done | bytes 131104 | tf_op jit(solution)/shard_map/ppermute | solution.py:20
  94.7 3.9 %all-to-all-start = ((bf16[8,80,256]{2,1,0:T(8,128)(2,1)}), bf16[8,80,256]{2,1,0:T(8,128)(2,1)S(1)}, u32[]{:S(2)}, u32[]{:S(2)}) async-start(bf16[8,80,256]{2,1,0:T(8,128)(2,1)} %get-tuple-element.102), calls=%async_computation | async-start | bytes 655360 | tf_op jit(solution)/shard_map/all_to_all | solution.py:481
  98.6 2.9 %collective-permute-start.36 = (bf16[128,512]{1,0:T(8,128)(2,1)S(1)}, bf16[128,512]{1,0:T(8,128)(2,1)S(1)}, u32[]{:S(2)}, u32[]{:S(2)}) collective-permute-start(bf16[128,512]{1,0:T(8,128)(2,1)S(1)} %get-tuple-element.106.refs_0_), channel_id=1, source_target_pairs={{0,16},{4,20},{8,24},{12,28},{16,0},{20,4},{24,8},{28,12},{1,17},{... | collective-permute-start | bytes 393224 | tf_op jit(solution)/shard_map/ppermute | solution.py:20
  101.5 13.3 %collective-permute-done.36.refs_1_ = bf16[128,512]{1,0:T(8,128)(2,1)S(1)} collective-permute-done((bf16[128,512]{1,0:T(8,128)(2,1)S(1)}, bf16[128,512]{1,0:T(8,128)(2,1)S(1)}, u32[]{:S(2)}, u32[]{:S(2)}) %collective-permute-start.36) | collective-permute-done | bytes 131104 | tf_op jit(solution)/shard_map/ppermute | solution.py:20
  116.5 5.7 %collective-permute-done.37.refs_1_ = bf16[256,512]{1,0:T(8,128)(2,1)} collective-permute-done((bf16[256,512]{1,0:T(8,128)(2,1)S(1)}, bf16[256,512]{1,0:T(8,128)(2,1)}, u32[]{:S(2)}, u32[]{:S(2)}) %collective-permute-start.37) | collective-permute-done | bytes 262176 | tf_op jit(solution)/shard_map/ppermute | solution.py:20
  134.9 4.2 %shard_map.207 = (bf16[2048,256]{1,0:T(8,128)(2,1)}, bf16[2048,256]{1,0:T(8,128)(2,1)}, bf16[256,2048]{1,0:T(8,128)(2,1)}) custom-call(bf16[256,1024]{1,0:T(8,128)(2,1)S(1)} %copy-done.16, bf16[256,1024]{1,0:T(8,128)(2,1)S(1)} %copy-done.18, bf16[256,1024]{1,0:T(8,128)(2,1)S(1)} %copy-done.20, bf16[256,1024]{1,0:T(8,128)(2,1)S(1)} %copy-done.22, ...), custom_call_target="tpu_custom_call" | custom-call | flops 1610612736 | bytes 8126464 | tf_op jit(solution)/shard_map/pallas_call | solution.py:37
  140.3 2.3 %shard_map.217 = f32[256,512]{1,0:T(8,128)} custom-call(bf16[8,80,256]{2,1,0:T(8,128)(2,1)S(1)} %all-to-all-done.own_ref.got_ref, bf16[8,80,256]{2,1,0:T(8,128)(2,1)S(1)} %collective-permute-done.35.other_ref, bf16[256,512]{1,0:T(8,128)(2,1)S(1)} %shard_map.216.refs_0_, bf16[256,512]{1,0:T(8,128)(2,1)} %collective-permute-done.37.refs_1_, ...), custom_call_target="tpu_custom_call" | custom-call | flops 268435456 | bytes 2228224 | tf_op jit(solution)/shard_map/pallas_call | solution.py:37
  (169 shorter events, 46.3 us)
Async XLA Ops:
  3.4 8.6 %collective-permute-start.4 = (bf16[64,1024]{1,0:T(8,128)(2,1)}, bf16[64,1024]{1,0:T(8,128)(2,1)S(1)}, u32[]{:S(2)}, u32[]{:S(2)}) collective-permute-start(bf16[64,1024]{1,0:T(8,128)(2,1)} %get-tuple-element.58), channel_id=1, source_target_pairs={{0,8},{4,12},{8,0},{12,4},{16,24},{20,28},{24,16},{28,20},{1,9},{5... | collective-permute-start | bytes 393224 | tf_op jit(solution)/shard_map/ppermute | solution.py:20
  6.5 10.4 %collective-permute-start.5 = (bf16[64,1024]{1,0:T(8,128)(2,1)}, bf16[64,1024]{1,0:T(8,128)(2,1)S(1)}, u32[]{:S(2)}, u32[]{:S(2)}) collective-permute-start(bf16[64,1024]{1,0:T(8,128)(2,1)} %get-tuple-element.59), channel_id=1, source_target_pairs={{0,12},{4,8},{8,4},{12,0},{16,28},{20,24},{24,20},{28,16},{1,13},{... | collective-permute-start | bytes 393224 | tf_op jit(solution)/shard_map/ppermute | solution.py:20
  7.9 10.6 %collective-permute-start = (bf16[64,1024]{1,0:T(8,128)(2,1)}, bf16[64,1024]{1,0:T(8,128)(2,1)S(1)}, u32[]{:S(2)}, u32[]{:S(2)}) collective-permute-start(bf16[64,1024]{1,0:T(8,128)(2,1)} %get-tuple-element.57), channel_id=1, source_target_pairs={{0,4},{4,0},{8,12},{12,8},{16,20},{20,16},{24,28},{28,24},{1,5},{5... | collective-permute-start | bytes 393224 | tf_op jit(solution)/shard_map/ppermute | solution.py:20
  8.1 16.8 %collective-permute-start.10 = (bf16[64,1024]{1,0:T(8,128)(2,1)}, bf16[64,1024]{1,0:T(8,128)(2,1)S(1)}, u32[]{:S(2)}, u32[]{:S(2)}) collective-permute-start(bf16[64,1024]{1,0:T(8,128)(2,1)} %get-tuple-element.65), channel_id=1, source_target_pairs={{0,20},{4,16},{8,28},{12,24},{16,4},{20,0},{24,12},{28,8},{1,21},{... | collective-permute-start | bytes 393224 | tf_op jit(solution)/shard_map/ppermute | solution.py:20
  17.0 19.7 %collective-permute-start.7 = (bf16[128,1024]{1,0:T(8,128)(2,1)S(1)}, bf16[128,1024]{1,0:T(8,128)(2,1)S(1)}, u32[]{:S(2)}, u32[]{:S(2)}) collective-permute-start(bf16[128,1024]{1,0:T(8,128)(2,1)S(1)} %shard_map.201.refs_4_), channel_id=1, source_target_pairs={{0,2},{1,3},{2,0},{3,1},{4,6},{5,7},{6,4},{7,5},{8,10},{9,11},{10,... | collective-permute-start | bytes 786440 | tf_op jit(solution)/shard_map/ppermute | solution.py:20
  19.5 17.2 %collective-permute-start.2 = (bf16[128,1024]{1,0:T(8,128)(2,1)S(1)}, bf16[128,1024]{1,0:T(8,128)(2,1)S(1)}, u32[]{:S(2)}, u32[]{:S(2)}) collective-permute-start(bf16[128,1024]{1,0:T(8,128)(2,1)S(1)} %shard_map.200.refs_0_), channel_id=1, source_target_pairs={{0,2},{1,3},{2,0},{3,1},{4,6},{5,7},{6,4},{7,5},{8,10},{9,11},{10,... | collective-permute-start | bytes 786440 | tf_op jit(solution)/shard_map/ppermute | solution.py:20
  20.9 14.5 %collective-permute-start.9 = (bf16[64,1024]{1,0:T(8,128)(2,1)}, bf16[64,1024]{1,0:T(8,128)(2,1)S(1)}, u32[]{:S(2)}, u32[]{:S(2)}) collective-permute-start(bf16[64,1024]{1,0:T(8,128)(2,1)} %get-tuple-element.64), channel_id=1, source_target_pairs={{0,16},{4,20},{8,24},{12,28},{16,0},{20,4},{24,8},{28,12},{1,17},{... | collective-permute-start | bytes 393224 | tf_op jit(solution)/shard_map/ppermute | solution.py:20
  23.5 11.9 %collective-permute-start.14 = (bf16[64,1024]{1,0:T(8,128)(2,1)}, bf16[64,1024]{1,0:T(8,128)(2,1)S(1)}, u32[]{:S(2)}, u32[]{:S(2)}) collective-permute-start(bf16[64,1024]{1,0:T(8,128)(2,1)} %get-tuple-element.66), channel_id=1, source_target_pairs={{0,24},{4,28},{8,16},{12,20},{16,8},{20,12},{24,0},{28,4},{1,25},{... | collective-permute-start | bytes 393224 | tf_op jit(solution)/shard_map/ppermute | solution.py:20
  24.9 11.2 %collective-permute-start.15 = (bf16[64,1024]{1,0:T(8,128)(2,1)}, bf16[64,1024]{1,0:T(8,128)(2,1)S(1)}, u32[]{:S(2)}, u32[]{:S(2)}) collective-permute-start(bf16[64,1024]{1,0:T(8,128)(2,1)} %get-tuple-element.67), channel_id=1, source_target_pairs={{0,28},{4,24},{8,20},{12,16},{16,12},{20,8},{24,4},{28,0},{1,29},{... | collective-permute-start | bytes 393224 | tf_op jit(solution)/shard_map/ppermute | solution.py:20
  36.0 9.2 %collective-permute-start.12 = (bf16[128,1024]{1,0:T(8,128)(2,1)S(1)}, bf16[128,1024]{1,0:T(8,128)(2,1)S(1)}, u32[]{:S(2)}, u32[]{:S(2)}) collective-permute-start(bf16[128,1024]{1,0:T(8,128)(2,1)S(1)} %shard_map.203.refs_0_.refs_4_), channel_id=1, source_target_pairs={{0,2},{1,3},{2,0},{3,1},{4,6},{5,7},{6,4},{7,5},{8,10},{9,11},{10,... | collective-permute-start | bytes 786440 | tf_op jit(solution)/shard_map/ppermute | solution.py:20
  36.7 8.5 %collective-permute-start.8 = (bf16[128,1024]{1,0:T(8,128)(2,1)S(1)}, bf16[128,1024]{1,0:T(8,128)(2,1)S(1)}, u32[]{:S(2)}, u32[]{:S(2)}) collective-permute-start(bf16[128,1024]{1,0:T(8,128)(2,1)S(1)} %collective-permute-done.7.refs_6_), channel_id=1, source_target_pairs={{0,1},{1,0},{2,3},{3,2},{4,5},{5,4},{6,7},{7,6},{8,9},{9,8},{10,11... | collective-permute-start | bytes 786440 | tf_op jit(solution)/shard_map/ppermute | solution.py:20
  37.2 12.9 %collective-permute-start.17 = (bf16[128,1024]{1,0:T(8,128)(2,1)S(1)}, bf16[128,1024]{1,0:T(8,128)(2,1)S(1)}, u32[]{:S(2)}, u32[]{:S(2)}) collective-permute-start(bf16[128,1024]{1,0:T(8,128)(2,1)S(1)} %shard_map.204.refs_0_.refs_8_), channel_id=1, source_target_pairs={{0,2},{1,3},{2,0},{3,1},{4,6},{5,7},{6,4},{7,5},{8,10},{9,11},{10,... | collective-permute-start | bytes 786440 | tf_op jit(solution)/shard_map/ppermute | solution.py:20
  38.7 11.9 %collective-permute-start.11 = (bf16[128,1024]{1,0:T(8,128)(2,1)S(1)}, bf16[128,1024]{1,0:T(8,128)(2,1)S(1)}, u32[]{:S(2)}, u32[]{:S(2)}) collective-permute-start(bf16[128,1024]{1,0:T(8,128)(2,1)S(1)} %shard_map.203.refs_0_.refs_4_), channel_id=1, source_target_pairs={{0,1},{1,0},{2,3},{3,2},{4,5},{5,4},{6,7},{7,6},{8,9},{9,8},{10,11... | collective-permute-start | bytes 786440 | tf_op jit(solution)/shard_map/ppermute | solution.py:20
  56.6 8.7 %collective-permute-start.20 = (bf16[64,1024]{1,0:T(8,128)(2,1)S(1)}, bf16[64,1024]{1,0:T(8,128)(2,1)S(1)}, u32[]{:S(2)}, u32[]{:S(2)}) collective-permute-start(bf16[64,1024]{1,0:T(8,128)(2,1)S(1)} %get-tuple-element.84), channel_id=1, source_target_pairs={{0,4},{4,0},{8,12},{12,8},{16,20},{20,16},{24,28},{28,24},{1,5},{5... | collective-permute-start | bytes 393224 | tf_op jit(solution)/shard_map/ppermute | solution.py:20
  57.1 10.3 %collective-permute-start.21 = (bf16[64,1024]{1,0:T(8,128)(2,1)S(1)}, bf16[64,1024]{1,0:T(8,128)(2,1)S(1)}, u32[]{:S(2)}, u32[]{:S(2)}) collective-permute-start(bf16[64,1024]{1,0:T(8,128)(2,1)S(1)} %get-tuple-element.85), channel_id=1, source_target_pairs={{0,8},{4,12},{8,0},{12,4},{16,24},{20,28},{24,16},{28,20},{1,9},{5... | collective-permute-start | bytes 393224 | tf_op jit(solution)/shard_map/ppermute | solution.py:20
  63.7 11.2 %collective-permute-start.25 = (bf16[128,512]{1,0:T(8,128)(2,1)S(1)}, bf16[128,512]{1,0:T(8,128)(2,1)S(1)}, u32[]{:S(2)}, u32[]{:S(2)}) collective-permute-start(bf16[128,512]{1,0:T(8,128)(2,1)S(1)} %get-tuple-element.92), channel_id=1, source_target_pairs={{0,2},{1,3},{2,0},{3,1},{4,6},{5,7},{6,4},{7,5},{8,10},{9,11},{10,... | collective-permute-start | bytes 393224 | tf_op jit(solution)/shard_map/ppermute | solution.py:20
  69.4 15.8 %collective-permute-start.23 = (bf16[128,512]{1,0:T(8,128)(2,1)S(1)}, bf16[128,512]{1,0:T(8,128)(2,1)S(1)}, u32[]{:S(2)}, u32[]{:S(2)}) collective-permute-start(bf16[128,512]{1,0:T(8,128)(2,1)S(1)} %get-tuple-element.88), channel_id=1, source_target_pairs={{0,2},{1,3},{2,0},{3,1},{4,6},{5,7},{6,4},{7,5},{8,10},{9,11},{10,... | collective-permute-start | bytes 393224 | tf_op jit(solution)/shard_map/ppermute | solution.py:20
  75.0 9.0 %collective-permute-start.26 = (bf16[64,512]{1,0:T(8,128)(2,1)S(1)}, bf16[64,512]{1,0:T(8,128)(2,1)S(1)}, u32[]{:S(2)}, u32[]{:S(2)}) collective-permute-start(bf16[64,512]{1,0:T(8,128)(2,1)S(1)} %get-tuple-element.93), channel_id=1, source_target_pairs={{0,16},{4,20},{8,24},{12,28},{16,0},{20,4},{24,8},{28,12},{1,17},{... | collective-permute-start | bytes 196616 | tf_op jit(solution)/shard_map/ppermute | solution.py:20
  76.4 8.8 %collective-permute-start.27 = (bf16[64,512]{1,0:T(8,128)(2,1)S(1)}, bf16[64,512]{1,0:T(8,128)(2,1)S(1)}, u32[]{:S(2)}, u32[]{:S(2)}) collective-permute-start(bf16[64,512]{1,0:T(8,128)(2,1)S(1)} %get-tuple-element.94), channel_id=1, source_target_pairs={{0,20},{4,16},{8,28},{12,24},{16,4},{20,0},{24,12},{28,8},{1,21},{... | collective-permute-start | bytes 196616 | tf_op jit(solution)/shard_map/ppermute | solution.py:20
  94.7 20.2 %all-to-all-start = ((bf16[8,80,256]{2,1,0:T(8,128)(2,1)}), bf16[8,80,256]{2,1,0:T(8,128)(2,1)S(1)}, u32[]{:S(2)}, u32[]{:S(2)}) async-start(bf16[8,80,256]{2,1,0:T(8,128)(2,1)} %get-tuple-element.102), calls=%async_computation | async-start | bytes 655360 | tf_op jit(solution)/shard_map/all_to_all | solution.py:481
  98.6 16.2 %collective-permute-start.36 = (bf16[128,512]{1,0:T(8,128)(2,1)S(1)}, bf16[128,512]{1,0:T(8,128)(2,1)S(1)}, u32[]{:S(2)}, u32[]{:S(2)}) collective-permute-start(bf16[128,512]{1,0:T(8,128)(2,1)S(1)} %get-tuple-element.106.refs_0_), channel_id=1, source_target_pairs={{0,16},{4,20},{8,24},{12,28},{16,0},{20,4},{24,8},{28,12},{1,17},{... | collective-permute-start | bytes 393224 | tf_op jit(solution)/shard_map/ppermute | solution.py:20
  114.9 25.4 %collective-permute-start.35 = (bf16[8,80,256]{2,1,0:T(8,128)(2,1)S(1)}, bf16[8,80,256]{2,1,0:T(8,128)(2,1)S(1)}, u32[]{:S(2)}, u32[]{:S(2)}) collective-permute-start(bf16[8,80,256]{2,1,0:T(8,128)(2,1)S(1)} %all-to-all-done.own_ref.got_ref), channel_id=1, source_target_pairs={{0,1},{1,0},{2,3},{3,2},{4,5},{5,4},{6,7},{7,6},{8,9},{9,8},{10,11... | collective-permute-start | bytes 983048 | tf_op jit(solution)/shard_map/ppermute | solution.py:20
  114.9 25.3 %collective-permute-start.38 = (bf16[256,512]{1,0:T(8,128)(2,1)S(1)}, bf16[256,512]{1,0:T(8,128)(2,1)S(1)}, u32[]{:S(2)}, u32[]{:S(2)}) collective-permute-start(bf16[256,512]{1,0:T(8,128)(2,1)S(1)} %shard_map.216.refs_0_), channel_id=1, source_target_pairs={{0,4},{4,0},{8,12},{12,8},{16,20},{20,16},{24,28},{28,24},{1,5},{5... | collective-permute-start | bytes 786440 | tf_op jit(solution)/shard_map/ppermute | solution.py:20
  122.2 18.1 %collective-permute-start.39 = (bf16[256,512]{1,0:T(8,128)(2,1)}, bf16[256,512]{1,0:T(8,128)(2,1)S(1)}, u32[]{:S(2)}, u32[]{:S(2)}) collective-permute-start(bf16[256,512]{1,0:T(8,128)(2,1)} %collective-permute-done.37.refs_1_), channel_id=1, source_target_pairs={{0,4},{4,0},{8,12},{12,8},{16,20},{20,16},{24,28},{28,24},{1,5},{5... | collective-permute-start | bytes 786440 | tf_op jit(solution)/shard_map/ppermute | solution.py:20
  (61 other events, 545.3 us)

commit v2 on v1

--- a/solution.py
+++ b/solution.py
@@ -49,16 +49,18 @@
     return jax.ShapeDtypeStruct(shape, dtype)
 
 
-def dispatch_kernel(n, cap, *refs):
-    d_ref, first_ref, blocks = refs[4], refs[5], refs[6 : 6 + n]
-    held, sems = refs[6 + n : 10 + n], refs[10 + n]
+def dispatch_kernel(n, cap, own, *refs):
     me = lax.axis_index("sp")
-    copies = [pltpu.make_async_copy(refs[i], held[i], sems.at[i]) for i in range(4)]
-    for copy in copies:
-        copy.start()
-    for copy in copies:
-        copy.wait()
-    ids_ref, w_ref, x_ref, g_ref = held
+    inputs, blocks, slots = refs[:4], refs[4:], n * cap // 2
+    if own:
+        d_ref, first_ref, blocks, sems = refs[4], refs[5], refs[6:-5], refs[-1]
+        copies = [pltpu.make_async_copy(refs[i], refs[i - 5], sems.at[i]) for i in range(4)]
+        for copy in copies:
+            copy.start()
+        for copy in copies:
+            copy.wait()
+        inputs, slots = refs[-5:-1], n * cap
+    ids_ref, w_ref, x_ref, g_ref = inputs
     tok, feat = x_ref.shape
     ids = ids_ref[...] ^ me
     who = lax.broadcasted_iota(jnp.int32, (n, tok), 0)
@@ -72,14 +74,16 @@
     before[1] = before[1] + jnp.sum(one[0], axis=1, keepdims=True)
     rank = [jnp.sum(b * o, axis=0, keepdims=True) for b, o in zip(before, one)]
     pos = [ids[k : k + 1, :] * cap + rank[k].astype(jnp.int32) for k in range(2)]
-    slot = lax.broadcasted_iota(jnp.int32, (n * cap, tok), 0)
+    slot = lax.broadcasted_iota(jnp.int32, (slots, tok), 0)
     hit = [slot == p for p in pos]
     weight = jnp.where(hit[0], w_ref[0:1, :], 0.0) + jnp.where(hit[1], w_ref[1:2, :], 0.0)
     weight = jnp.sum(weight, axis=1, keepdims=True)
     pick = jnp.where(hit[0] | hit[1], 1.0, 0.0).astype(BF)
-    d_ref[...] = pick
-    row = lax.broadcasted_iota(jnp.int32, first_ref.shape, 0)
-    first_ref[...] = jnp.where((row == 0) & (me == 0), 1.0, 0.0)
+    if own:
+        d_ref[...] = pick
+        row = lax.broadcasted_iota(jnp.int32, first_ref.shape, 0)
+        first_ref[...] = jnp.where((row == 0) & (me == 0), 1.0, 0.0)
+        pick, weight = pick[: slots // 2], weight[: slots // 2]
     rows = dot(pick, x_ref[...]).astype(BF)
     cots = (dot(pick, g_ref[...]) * weight).astype(BF)
     for k, block in enumerate(blocks):
@@ -127,19 +131,24 @@
     me = lax.axis_index("tp")
     parts = [refs[h * m : (h + 1) * m] for h in range(chunks)]
     grads = refs[chunks * m : chunks * (m + 3)]
-    gg_ref, gu_ref, gd_ref = refs[-3:]
-    feat = parts[0][0].shape[1] // 2
+    gg_ref, gu_ref, gd_ref, rows_ref, both_ref, act_ref = refs[-6:]
+    feat, hidden = parts[0][0].shape[1] // 2, gg_ref.shape[1]
+    spans, at = [], 0
+    for h in range(chunks):
+        spans.append(slice(at, at + parts[h][0].shape[0]))
+        at = spans[-1].stop
+        both_ref[spans[h], :hidden] = grads[3 * h][...]
+        both_ref[spans[h], hidden:] = grads[3 * h + 1][...]
+        act_ref[spans[h], :] = grads[3 * h + 2][...]
+    active = act_ref[...].T
     for q in range(m):
         span = pl.ds(pl.multiple_of((me ^ q) * feat, feat), feat)
-        gate = up = down = 0.0
         for h in range(chunks):
-            rows = parts[h][q][:, :feat]
-            gate += dot_tn(rows, grads[3 * h][...])
-            up += dot_tn(rows, grads[3 * h + 1][...])
-            down += dot_tn(grads[3 * h + 2][...], parts[h][q][:, feat:])
-        gg_ref[span, :] = gate.astype(BF)
-        gu_ref[span, :] = up.astype(BF)
-        gd_ref[:, span] = down.astype(BF)
+            rows_ref[spans[h], :] = parts[h][q][...]
+        both = dot_tn(rows_ref[:, :feat], both_ref[...]).astype(BF)
+        gg_ref[span, :] = both[:, :hidden]
+        gu_ref[span, :] = both[:, hidden:]
+        gd_ref[:, span] = dot(active, rows_ref[:, feat:]).astype(BF)
 
 
 def join_kernel(*refs):
@@ -301,12 +310,15 @@
     hidden = wg.shape[1]
     channels = conv_out.shape[1]
 
+    sources = [route_ids.T, route_weights.T, mixer_out, cotangent]
+    passed = [hop(source, "sp", n // 2) for source in sources]
     sent = call(
-        functools.partial(dispatch_kernel, n, cap),
-        [struct((slots, tok), BF), struct((tok, 128), F32)] + [struct((cap, 2 * feat), BF)] * n,
-        [route_ids.T, route_weights.T, mixer_out, cotangent],
+        functools.partial(dispatch_kernel, n, cap, True),
+        [struct((slots, tok), BF), struct((tok, 128), F32)]
+        + [struct((cap, 2 * feat), BF)] * (n // 2),
+        sources,
         [HB] * 4,
-        4 * slots * tok * feat,
+        2 * slots * tok * feat,
         scratch=[
             pltpu.VMEM((2, tok), jnp.int32),
             pltpu.VMEM((2, tok), F32),
@@ -317,9 +329,19 @@
         limit=60,
     )
     pick, first, sent = sent[0], sent[1], sent[2:]
+    relayed = call(
+        functools.partial(dispatch_kernel, n, cap, False),
+        [struct((cap, 2 * feat), BF)] * (n // 2),
+        passed,
+        [VM] * 4,
+        2 * slots * tok * feat,
+    )
     edges = [0, n // 4, n // 2, 3 * n // 4, n]
     chunks = [range(a, b) for a, b in zip(edges, edges[1:])]
-    got = [sent[0]] + [hop(sent[k], "sp", k) for k in range(1, n)]
+    got = []
+    for k in range(n):
+        block = sent[k] if k < n // 2 else relayed[k - n // 2]
+        got.append(hop(block, "sp", k % (n // 2)) if k % (n // 2) else block)
 
     rate = decay_rate[None, :]
     recur_f = recur_gate.astype(F32)
@@ -428,7 +450,12 @@
         [a for piece in parts for a in piece] + [a for g in grads for a in g],
         [VM] * (len(parts) * (m + 3)),
         6 * slots * m * feat * hidden,
-        limit=24,
+        scratch=[
+            pltpu.VMEM((slots, 2 * feat), BF),
+            pltpu.VMEM((slots, 2 * hidden), BF),
+            pltpu.VMEM((slots, hidden), BF),
+        ],
+        limit=16,
     )
 
     near_rows = slots // 2

time: 143 us -> 137 us (0.958)
  starting transfers between devices: 51.3 us -> 47.1 us
  waiting for transfers between devices: 53.8 us -> 51.4 us
    ppermute x40 -> x43, starting transfers between devices: 47.5 us -> 43.5 us  [hop(): return lax.ppermute(value, axis, [(i, i ^ bit) for i in range(count)])]
    ppermute x40 -> x43, waiting for transfers between devices: 53.8 us -> 51.4 us  [hop(): return lax.ppermute(value, axis, [(i, i ^ bit) for i in range(count)])]
    pallas_call x20 -> x21, Pallas kernels: 18.8 us -> 18 us  [call(): pl.pallas_call(kernel, out_shape=list(outs), in_specs=specs, out_specs=[V...]
  transfers between devices with their start and end apart: 41 -> 44, of which waited for: 12 -> 15; matrix products, arithmetic and copies ran while one was open for 1% -> 1% of each run, Pallas kernels for 8% -> 9%
where the time goes in v2:
time: 137 us; the launch traced here: 136 us
  waiting for transfers between devices  51.4 us (38%)
  starting transfers between devices  47.1 us (34%)
  Pallas kernels  18 us (13%)
  local copies, waits for them, and re-layouts  17.4 us (13%)
    ppermute x43, waiting for transfers between devices, hop(): return lax.ppermute(value, axis, [(i, i ^ bit) for i in range(count)])  51.4 us
    ppermute x43, starting transfers between devices, hop(): return lax.ppermute(value, axis, [(i, i ^ bit) for i in range(count)])  43.5 us
    pallas_call x21, Pallas kernels, call(): pl.pallas_call(kernel, out_shape=list(outs), in_specs=specs, out_specs=[V...  18 us
    unnamed x88, local copies, waits for them, and re-layouts  17.4 us
    all_to_all x1, starting transfers between devices, body(): own = lax.all_to_all(slices, 'sp', split_axis=0, concat_axis=0, tiled=True)  3.61 us
  transfers between devices with their start and end apart: 44, of which 15 were waited for; matrix products, arithmetic and copies ran while one was open for 1% of the time, Pallas kernels for 9%

profile of v2, /device:TPU:0, one launch (start us, length us, event | category | flops | bytes accessed | tf_op | source)
XLA Modules:
  0.0 135.7 jit_solution(4769641675865669431)
XLA Ops:
  0.7 2.4 %shard_map.199 = (bf16[512,128]{1,0:T(8,128)(2,1)}, f32[128,128]{1,0:T(8,128)}, bf16[64,1024]{1,0:T(8,128)(2,1)}, bf16[64,1024]{1,0:T(8,128)(2,1)}, bf16[64,1024]{1,0:T(8,128)(2,1)}, /*index=5*/bf16[64,1024]{1,0:T(8,128)(2,1)}) custom-call(s32[2,128]{1,0:T(2,128)} %bitcast.19, f32[2,128]{1,0:T(2,128)} %bitcast.17, bf16[128,512]{1,0:T(8,128)(2,1)} %refs_2_.1, ...), custom_call_target="tpu_custom_call" | custom-call | flops 67108864 | bytes 985088 | tf_op jit(solution)/shard_map/pallas_call | solution.py:37
  3.0 3.1 %collective-permute-start.4 = (bf16[64,1024]{1,0:T(8,128)(2,1)}, bf16[64,1024]{1,0:T(8,128)(2,1)S(1)}, u32[]{:S(2)}, u32[]{:S(2)}) collective-permute-start(bf16[64,1024]{1,0:T(8,128)(2,1)} %get-tuple-element.58), channel_id=1, source_target_pairs={{0,8},{4,12},{8,0},{12,4},{16,24},{20,28},{24,16},{28,20},{1,9},{5... | collective-permute-start | bytes 393224 | tf_op jit(solution)/shard_map/ppermute | solution.py:20
  7.7 3.0 %collective-permute-start.11 = (bf16[128,512]{1,0:T(8,128)(2,1)}, bf16[128,512]{1,0:T(8,128)(2,1)S(1)}, u32[]{:S(2)}, u32[]{:S(2)}) collective-permute-start(bf16[128,512]{1,0:T(8,128)(2,1)} %refs_2_.1), channel_id=1, source_target_pairs={{0,16},{4,20},{8,24},{12,28},{16,0},{20,4},{24,8},{28,12},{1,17},{... | collective-permute-start | bytes 393224 | tf_op jit(solution)/shard_map/ppermute | solution.py:20
  10.7 2.9 %collective-permute-start.10 = (f32[2,128]{1,0:T(2,128)}, f32[2,128]{1,0:T(2,128)S(1)}, u32[]{:S(2)}, u32[]{:S(2)}) collective-permute-start(f32[2,128]{1,0:T(2,128)} %bitcast.18), channel_id=1, source_target_pairs={{0,16},{4,20},{8,24},{12,28},{16,0},{20,4},{24,8},{28,12},{1,17},{... | collective-permute-start | bytes 3080 | tf_op jit(solution)/shard_map/ppermute | solution.py:20
  13.6 3.7 %collective-permute-done.5.refs_1_ = bf16[64,1024]{1,0:T(8,128)(2,1)S(1)} collective-permute-done((bf16[64,1024]{1,0:T(8,128)(2,1)}, bf16[64,1024]{1,0:T(8,128)(2,1)S(1)}, u32[]{:S(2)}, u32[]{:S(2)}) %collective-permute-start.5) | collective-permute-done | bytes 131104 | tf_op jit(solution)/shard_map/ppermute | solution.py:20
  20.0 2.3 %collective-permute-done.10.refs_1_ = f32[2,128]{1,0:T(2,128)S(1)} collective-permute-done((f32[2,128]{1,0:T(2,128)}, f32[2,128]{1,0:T(2,128)S(1)}, u32[]{:S(2)}, u32[]{:S(2)}) %collective-permute-start.10) | collective-permute-done | bytes 1056 | tf_op jit(solution)/shard_map/ppermute | solution.py:20
  28.2 2.9 %collective-permute-done.13.refs_1_ = bf16[64,1024]{1,0:T(8,128)(2,1)S(1)} collective-permute-done((bf16[64,1024]{1,0:T(8,128)(2,1)S(1)}, bf16[64,1024]{1,0:T(8,128)(2,1)S(1)}, u32[]{:S(2)}, u32[]{:S(2)}) %collective-permute-start.13) | collective-permute-done | bytes 131104 | tf_op jit(solution)/shard_map/ppermute | solution.py:20
  35.5 6.5 %collective-permute-done.15.refs_2_.refs_6_ = bf16[128,1024]{1,0:T(8,128)(2,1)S(1)} collective-permute-done((bf16[128,1024]{1,0:T(8,128)(2,1)S(1)}, bf16[128,1024]{1,0:T(8,128)(2,1)S(1)}, u32[]{:S(2)}, u32[]{:S(2)}) %collective-permute-start.15) | collective-permute-done | bytes 262176 | tf_op jit(solution)/shard_map/ppermute | solution.py:20
  43.3 2.2 %shard_map.202 = (bf16[256,256]{1,0:T(8,128)(2,1)S(1)}, bf16[256,256]{1,0:T(8,128)(2,1)S(1)}, bf16[256,256]{1,0:T(8,128)(2,1)S(1)}, bf16[256,1024]{1,0:T(8,128)(...) custom-call(bf16[128,1024]{1,0:T(8,128)(2,1)S(1)} %shard_map.200.ref, ...), custom_call_target="tpu_custom_call" | custom-call | flops 1342177280 | bytes 8781824 | tf_op jit(solution)/shard_map/pallas_call | solution.py:37
  47.4 1.9 %shard_map.206 = (bf16[128,256]{1,0:T(8,128)(2,1)S(1)}, bf16[128,256]{1,0:T(8,128)(2,1)S(1)}, bf16[128,256]{1,0:T(8,128)(2,1)S(1)}, bf16[128,1024]{1,0:T(8,128)(2,1)S(1)}, bf16[128,1024]{1,0:T(8,128)(2,1)S(1)}) custom-call(bf16[128,1024]{1,0:T(8,128)(2,1)S(1)} %shard_map.204.refs_0_.refs_4_, bf16[128,1024]{1,0:T(8,128)(2,1)S(1)} %collective-permute-done.14.refs_1_.refs_5_, ...), custom_call_target="tpu_custom_call" | custom-call | flops 671088640 | bytes 5046272 | tf_op jit(solution)/shard_map/pallas_call | solution.py:37
  50.0 1.9 %shard_map.207 = (bf16[128,256]{1,0:T(8,128)(2,1)S(1)}, bf16[128,256]{1,0:T(8,128)(2,1)S(1)}, bf16[128,256]{1,0:T(8,128)(2,1)S(1)}, bf16[128,1024]{1,0:T(8,128)(2,1)S(1)}, bf16[128,1024]{1,0:T(8,128)(2,1)S(1)}) custom-call(bf16[128,1024]{1,0:T(8,128)(2,1)S(1)} %shard_map.205.refs_0_.refs_8_, bf16[128,1024]{1,0:T(8,128)(2,1)S(1)} %collective-permute-done.19.refs_1_.refs_9_, ...), custom_call_target="tpu_custom_call" | custom-call | flops 671088640 | bytes 4980736 | tf_op jit(solution)/shard_map/pallas_call | solution.py:37
  59.8 2.1 %collective-permute-done.24.refs_2_ = bf16[64,1024]{1,0:T(8,128)(2,1)S(1)} collective-permute-done((bf16[64,1024]{1,0:T(8,128)(2,1)S(1)}, bf16[64,1024]{1,0:T(8,128)(2,1)S(1)}, u32[]{:S(2)}, u32[]{:S(2)}) %collective-permute-start.24) | collective-permute-done | bytes 131104 | tf_op jit(solution)/shard_map/ppermute | solution.py:20
  64.3 2.9 %collective-permute-start.33 = (bf16[64,512]{1,0:T(8,128)(2,1)S(1)}, bf16[64,512]{1,0:T(8,128)(2,1)S(1)}, u32[]{:S(2)}, u32[]{:S(2)}) collective-permute-start(bf16[64,512]{1,0:T(8,128)(2,1)S(1)} %get-tuple-element.99), channel_id=1, source_target_pairs={{0,24},{4,28},{8,16},{12,20},{16,8},{20,12},{24,0},{28,4},{1,25},{... | collective-permute-start | bytes 196616 | tf_op jit(solution)/shard_map/ppermute | solution.py:20
  67.2 2.0 %collective-permute-start.34 = (bf16[64,512]{1,0:T(8,128)(2,1)S(1)}, bf16[64,512]{1,0:T(8,128)(2,1)S(1)}, u32[]{:S(2)}, u32[]{:S(2)}) collective-permute-start(bf16[64,512]{1,0:T(8,128)(2,1)S(1)} %get-tuple-element.100), channel_id=1, source_target_pairs={{0,28},{4,24},{8,20},{12,16},{16,12},{20,8},{24,4},{28,0},{1,29},{... | collective-permute-start | bytes 196616 | tf_op jit(solution)/shard_map/ppermute | solution.py:20
  69.4 2.7 %collective-permute-start.30 = (bf16[64,512]{1,0:T(8,128)(2,1)S(1)}, bf16[64,512]{1,0:T(8,128)(2,1)S(1)}, u32[]{:S(2)}, u32[]{:S(2)}) collective-permute-start(bf16[64,512]{1,0:T(8,128)(2,1)S(1)} %get-tuple-element.94), channel_id=1, source_target_pairs={{0,20},{4,16},{8,28},{12,24},{16,4},{20,0},{24,12},{28,8},{1,21},{... | collective-permute-start | bytes 196616 | tf_op jit(solution)/shard_map/ppermute | solution.py:20
  72.1 2.2 %collective-permute-done.34.refs_3_ = bf16[64,512]{1,0:T(8,128)(2,1)S(1)} collective-permute-done((bf16[64,512]{1,0:T(8,128)(2,1)S(1)}, bf16[64,512]{1,0:T(8,128)(2,1)S(1)}, u32[]{:S(2)}, u32[]{:S(2)}) %collective-permute-start.34) | collective-permute-done | bytes 65568 | tf_op jit(solution)/shard_map/ppermute | solution.py:20
  74.3 3.4 %collective-permute-done.29.refs_0_ = bf16[64,512]{1,0:T(8,128)(2,1)S(1)} collective-permute-done((bf16[64,512]{1,0:T(8,128)(2,1)S(1)}, bf16[64,512]{1,0:T(8,128)(2,1)S(1)}, u32[]{:S(2)}, u32[]{:S(2)}) %collective-permute-start.29) | collective-permute-done | bytes 65568 | tf_op jit(solution)/shard_map/ppermute | solution.py:20
  81.2 3.3 %collective-permute-done.36.refs_2_ = bf16[128,512]{1,0:T(8,128)(2,1)S(1)} collective-permute-done((bf16[128,512]{1,0:T(8,128)(2,1)S(1)}, bf16[128,512]{1,0:T(8,128)(2,1)S(1)}, u32[]{:S(2)}, u32[]{:S(2)}) %collective-permute-start.36) | collective-permute-done | bytes 131104 | tf_op jit(solution)/shard_map/ppermute | solution.py:20
  88.7 3.6 %all-to-all-start = ((bf16[8,80,256]{2,1,0:T(8,128)(2,1)}), bf16[8,80,256]{2,1,0:T(8,128)(2,1)S(1)}, u32[]{:S(2)}, u32[]{:S(2)}) async-start(bf16[8,80,256]{2,1,0:T(8,128)(2,1)} %get-tuple-element.102), calls=%async_computation | async-start | bytes 655360 | tf_op jit(solution)/shard_map/all_to_all | solution.py:508
  92.4 2.7 %collective-permute-start.39 = (bf16[128,512]{1,0:T(8,128)(2,1)S(1)}, bf16[128,512]{1,0:T(8,128)(2,1)S(1)}, u32[]{:S(2)}, u32[]{:S(2)}) collective-permute-start(bf16[128,512]{1,0:T(8,128)(2,1)S(1)} %get-tuple-element.106.refs_0_), channel_id=1, source_target_pairs={{0,16},{4,20},{8,24},{12,28},{16,0},{20,4},{24,8},{28,12},{1,17},{... | collective-permute-start | bytes 393224 | tf_op jit(solution)/shard_map/ppermute | solution.py:20
  95.0 13.5 %collective-permute-done.39.refs_1_ = bf16[128,512]{1,0:T(8,128)(2,1)S(1)} collective-permute-done((bf16[128,512]{1,0:T(8,128)(2,1)S(1)}, bf16[128,512]{1,0:T(8,128)(2,1)S(1)}, u32[]{:S(2)}, u32[]{:S(2)}) %collective-permute-start.39) | collective-permute-done | bytes 131104 | tf_op jit(solution)/shard_map/ppermute | solution.py:20
  110.3 6.0 %collective-permute-done.40.refs_1_ = bf16[256,512]{1,0:T(8,128)(2,1)} collective-permute-done((bf16[256,512]{1,0:T(8,128)(2,1)S(1)}, bf16[256,512]{1,0:T(8,128)(2,1)}, u32[]{:S(2)}, u32[]{:S(2)}) %collective-permute-start.40) | collective-permute-done | bytes 262176 | tf_op jit(solution)/shard_map/ppermute | solution.py:20
  128.9 3.4 %shard_map.208 = (bf16[2048,256]{1,0:T(8,128)(2,1)}, bf16[2048,256]{1,0:T(8,128)(2,1)}, bf16[256,2048]{1,0:T(8,128)(2,1)}) custom-call(bf16[256,1024]{1,0:T(8,128)(2,1)S(1)} %copy-done.16, bf16[256,1024]{1,0:T(8,128)(2,1)S(1)} %copy-done.18, bf16[256,1024]{1,0:T(8,128)(2,1)S(1)} %copy-done.20, bf16[256,1024]{1,0:T(8,128)(2,1)S(1)} %copy-done.22, ...), custom_call_target="tpu_custom_call" | custom-call | flops 1610612736 | bytes 8126464 | tf_op jit(solution)/shard_map/pallas_call | solution.py:37
  133.4 2.3 %shard_map.218 = f32[256,512]{1,0:T(8,128)} custom-call(bf16[8,80,256]{2,1,0:T(8,128)(2,1)S(1)} %all-to-all-done.own_ref.got_ref, bf16[8,80,256]{2,1,0:T(8,128)(2,1)S(1)} %collective-permute-done.38.other_ref, bf16[256,512]{1,0:T(8,128)(2,1)S(1)} %shard_map.217.refs_0_, bf16[256,512]{1,0:T(8,128)(2,1)} %collective-permute-done.40.refs_1_, ...), custom_call_target="tpu_custom_call" | custom-call | flops 268435456 | bytes 2228224 | tf_op jit(solution)/shard_map/pallas_call | solution.py:37
  (176 shorter events, 51.7 us)
Async XLA Ops:
  6.1 11.1 %collective-permute-start.5 = (bf16[64,1024]{1,0:T(8,128)(2,1)}, bf16[64,1024]{1,0:T(8,128)(2,1)S(1)}, u32[]{:S(2)}, u32[]{:S(2)}) collective-permute-start(bf16[64,1024]{1,0:T(8,128)(2,1)} %get-tuple-element.59), channel_id=1, source_target_pairs={{0,12},{4,8},{8,4},{12,0},{16,28},{20,24},{24,20},{28,16},{1,13},{... | collective-permute-start | bytes 393224 | tf_op jit(solution)/shard_map/ppermute | solution.py:20
  7.5 10.0 %collective-permute-start = (bf16[64,1024]{1,0:T(8,128)(2,1)}, bf16[64,1024]{1,0:T(8,128)(2,1)S(1)}, u32[]{:S(2)}, u32[]{:S(2)}) collective-permute-start(bf16[64,1024]{1,0:T(8,128)(2,1)} %get-tuple-element.57), channel_id=1, source_target_pairs={{0,4},{4,0},{8,12},{12,8},{16,20},{20,16},{24,28},{28,24},{1,5},{5... | collective-permute-start | bytes 393224 | tf_op jit(solution)/shard_map/ppermute | solution.py:20
  7.7 16.5 %collective-permute-start.11 = (bf16[128,512]{1,0:T(8,128)(2,1)}, bf16[128,512]{1,0:T(8,128)(2,1)S(1)}, u32[]{:S(2)}, u32[]{:S(2)}) collective-permute-start(bf16[128,512]{1,0:T(8,128)(2,1)} %refs_2_.1), channel_id=1, source_target_pairs={{0,16},{4,20},{8,24},{12,28},{16,0},{20,4},{24,8},{28,12},{1,17},{... | collective-permute-start | bytes 393224 | tf_op jit(solution)/shard_map/ppermute | solution.py:20
  10.6 13.6 %collective-permute-start.12 = (bf16[128,512]{1,0:T(8,128)(2,1)}, bf16[128,512]{1,0:T(8,128)(2,1)S(1)}, u32[]{:S(2)}, u32[]{:S(2)}) collective-permute-start(bf16[128,512]{1,0:T(8,128)(2,1)} %cot_ref.1), channel_id=1, source_target_pairs={{0,16},{4,20},{8,24},{12,28},{16,0},{20,4},{24,8},{28,12},{1,17},{... | collective-permute-start | bytes 393224 | tf_op jit(solution)/shard_map/ppermute | solution.py:20
  10.7 11.7 %collective-permute-start.10 = (f32[2,128]{1,0:T(2,128)}, f32[2,128]{1,0:T(2,128)S(1)}, u32[]{:S(2)}, u32[]{:S(2)}) collective-permute-start(f32[2,128]{1,0:T(2,128)} %bitcast.18), channel_id=1, source_target_pairs={{0,16},{4,20},{8,24},{12,28},{16,0},{20,4},{24,8},{28,12},{1,17},{... | collective-permute-start | bytes 3080 | tf_op jit(solution)/shard_map/ppermute | solution.py:20
  17.5 15.7 %collective-permute-start.7 = (bf16[128,1024]{1,0:T(8,128)(2,1)S(1)}, bf16[128,1024]{1,0:T(8,128)(2,1)S(1)}, u32[]{:S(2)}, u32[]{:S(2)}) collective-permute-start(bf16[128,1024]{1,0:T(8,128)(2,1)S(1)} %shard_map.201.refs_4_), channel_id=1, source_target_pairs={{0,2},{1,3},{2,0},{3,1},{4,6},{5,7},{6,4},{7,5},{8,10},{9,11},{10,... | collective-permute-start | bytes 786440 | tf_op jit(solution)/shard_map/ppermute | solution.py:20
  22.3 10.9 %collective-permute-start.2 = (bf16[128,1024]{1,0:T(8,128)(2,1)S(1)}, bf16[128,1024]{1,0:T(8,128)(2,1)S(1)}, u32[]{:S(2)}, u32[]{:S(2)}) collective-permute-start(bf16[128,1024]{1,0:T(8,128)(2,1)S(1)} %shard_map.200.refs_0_), channel_id=1, source_target_pairs={{0,2},{1,3},{2,0},{3,1},{4,6},{5,7},{6,4},{7,5},{8,10},{9,11},{10,... | collective-permute-start | bytes 786440 | tf_op jit(solution)/shard_map/ppermute | solution.py:20
  32.9 9.2 %collective-permute-start.15 = (bf16[128,1024]{1,0:T(8,128)(2,1)S(1)}, bf16[128,1024]{1,0:T(8,128)(2,1)S(1)}, u32[]{:S(2)}, u32[]{:S(2)}) collective-permute-start(bf16[128,1024]{1,0:T(8,128)(2,1)S(1)} %shard_map.204.refs_0_.refs_4_), channel_id=1, source_target_pairs={{0,2},{1,3},{2,0},{3,1},{4,6},{5,7},{6,4},{7,5},{8,10},{9,11},{10,... | collective-permute-start | bytes 786440 | tf_op jit(solution)/shard_map/ppermute | solution.py:20
  33.2 8.9 %collective-permute-start.8 = (bf16[128,1024]{1,0:T(8,128)(2,1)S(1)}, bf16[128,1024]{1,0:T(8,128)(2,1)S(1)}, u32[]{:S(2)}, u32[]{:S(2)}) collective-permute-start(bf16[128,1024]{1,0:T(8,128)(2,1)S(1)} %collective-permute-done.7.refs_6_), channel_id=1, source_target_pairs={{0,1},{1,0},{2,3},{3,2},{4,5},{5,4},{6,7},{7,6},{8,9},{9,8},{10,11... | collective-permute-start | bytes 786440 | tf_op jit(solution)/shard_map/ppermute | solution.py:20
  33.2 8.8 %collective-permute-start.3 = (bf16[128,1024]{1,0:T(8,128)(2,1)S(1)}, bf16[128,1024]{1,0:T(8,128)(2,1)S(1)}, u32[]{:S(2)}, u32[]{:S(2)}) collective-permute-start(bf16[128,1024]{1,0:T(8,128)(2,1)S(1)} %collective-permute-done.2.refs_2_), channel_id=1, source_target_pairs={{0,1},{1,0},{2,3},{3,2},{4,5},{5,4},{6,7},{7,6},{8,9},{9,8},{10,11... | collective-permute-start | bytes 786440 | tf_op jit(solution)/shard_map/ppermute | solution.py:20
  33.8 13.2 %collective-permute-start.20 = (bf16[128,1024]{1,0:T(8,128)(2,1)S(1)}, bf16[128,1024]{1,0:T(8,128)(2,1)S(1)}, u32[]{:S(2)}, u32[]{:S(2)}) collective-permute-start(bf16[128,1024]{1,0:T(8,128)(2,1)S(1)} %shard_map.205.refs_0_.refs_8_), channel_id=1, source_target_pairs={{0,2},{1,3},{2,0},{3,1},{4,6},{5,7},{6,4},{7,5},{8,10},{9,11},{10,... | collective-permute-start | bytes 786440 | tf_op jit(solution)/shard_map/ppermute | solution.py:20
  35.5 11.9 %collective-permute-start.14 = (bf16[128,1024]{1,0:T(8,128)(2,1)S(1)}, bf16[128,1024]{1,0:T(8,128)(2,1)S(1)}, u32[]{:S(2)}, u32[]{:S(2)}) collective-permute-start(bf16[128,1024]{1,0:T(8,128)(2,1)S(1)} %shard_map.204.refs_0_.refs_4_), channel_id=1, source_target_pairs={{0,1},{1,0},{2,3},{3,2},{4,5},{5,4},{6,7},{7,6},{8,9},{9,8},{10,11... | collective-permute-start | bytes 786440 | tf_op jit(solution)/shard_map/ppermute | solution.py:20
  55.9 7.7 %collective-permute-start.25 = (bf16[64,1024]{1,0:T(8,128)(2,1)S(1)}, bf16[64,1024]{1,0:T(8,128)(2,1)S(1)}, u32[]{:S(2)}, u32[]{:S(2)}) collective-permute-start(bf16[64,1024]{1,0:T(8,128)(2,1)S(1)} %get-tuple-element.86), channel_id=1, source_target_pairs={{0,12},{4,8},{8,4},{12,0},{16,28},{20,24},{24,20},{28,16},{1,13},{... | collective-permute-start | bytes 393224 | tf_op jit(solution)/shard_map/ppermute | solution.py:20
  58.1 11.2 %collective-permute-start.28 = (bf16[128,512]{1,0:T(8,128)(2,1)S(1)}, bf16[128,512]{1,0:T(8,128)(2,1)S(1)}, u32[]{:S(2)}, u32[]{:S(2)}) collective-permute-start(bf16[128,512]{1,0:T(8,128)(2,1)S(1)} %get-tuple-element.92), channel_id=1, source_target_pairs={{0,2},{1,3},{2,0},{3,1},{4,6},{5,7},{6,4},{7,5},{8,10},{9,11},{10,... | collective-permute-start | bytes 393224 | tf_op jit(solution)/shard_map/ppermute | solution.py:20
  63.8 15.4 %collective-permute-start.26 = (bf16[128,512]{1,0:T(8,128)(2,1)S(1)}, bf16[128,512]{1,0:T(8,128)(2,1)S(1)}, u32[]{:S(2)}, u32[]{:S(2)}) collective-permute-start(bf16[128,512]{1,0:T(8,128)(2,1)S(1)} %get-tuple-element.88), channel_id=1, source_target_pairs={{0,2},{1,3},{2,0},{3,1},{4,6},{5,7},{6,4},{7,5},{8,10},{9,11},{10,... | collective-permute-start | bytes 393224 | tf_op jit(solution)/shard_map/ppermute | solution.py:20
  64.3 7.8 %collective-permute-start.33 = (bf16[64,512]{1,0:T(8,128)(2,1)S(1)}, bf16[64,512]{1,0:T(8,128)(2,1)S(1)}, u32[]{:S(2)}, u32[]{:S(2)}) collective-permute-start(bf16[64,512]{1,0:T(8,128)(2,1)S(1)} %get-tuple-element.99), channel_id=1, source_target_pairs={{0,24},{4,28},{8,16},{12,20},{16,8},{20,12},{24,0},{28,4},{1,25},{... | collective-permute-start | bytes 196616 | tf_op jit(solution)/shard_map/ppermute | solution.py:20
  69.3 8.4 %collective-permute-start.29 = (bf16[64,512]{1,0:T(8,128)(2,1)S(1)}, bf16[64,512]{1,0:T(8,128)(2,1)S(1)}, u32[]{:S(2)}, u32[]{:S(2)}) collective-permute-start(bf16[64,512]{1,0:T(8,128)(2,1)S(1)} %get-tuple-element.93), channel_id=1, source_target_pairs={{0,16},{4,20},{8,24},{12,28},{16,0},{20,4},{24,8},{28,12},{1,17},{... | collective-permute-start | bytes 196616 | tf_op jit(solution)/shard_map/ppermute | solution.py:20
  69.4 9.9 %collective-permute-start.30 = (bf16[64,512]{1,0:T(8,128)(2,1)S(1)}, bf16[64,512]{1,0:T(8,128)(2,1)S(1)}, u32[]{:S(2)}, u32[]{:S(2)}) collective-permute-start(bf16[64,512]{1,0:T(8,128)(2,1)S(1)} %get-tuple-element.94), channel_id=1, source_target_pairs={{0,20},{4,16},{8,28},{12,24},{16,4},{20,0},{24,12},{28,8},{1,21},{... | collective-permute-start | bytes 196616 | tf_op jit(solution)/shard_map/ppermute | solution.py:20
  88.7 19.9 %all-to-all-start = ((bf16[8,80,256]{2,1,0:T(8,128)(2,1)}), bf16[8,80,256]{2,1,0:T(8,128)(2,1)S(1)}, u32[]{:S(2)}, u32[]{:S(2)}) async-start(bf16[8,80,256]{2,1,0:T(8,128)(2,1)} %get-tuple-element.102), calls=%async_computation | async-start | bytes 655360 | tf_op jit(solution)/shard_map/all_to_all | solution.py:508
  92.4 16.2 %collective-permute-start.39 = (bf16[128,512]{1,0:T(8,128)(2,1)S(1)}, bf16[128,512]{1,0:T(8,128)(2,1)S(1)}, u32[]{:S(2)}, u32[]{:S(2)}) collective-permute-start(bf16[128,512]{1,0:T(8,128)(2,1)S(1)} %get-tuple-element.106.refs_0_), channel_id=1, source_target_pairs={{0,16},{4,20},{8,24},{12,28},{16,0},{20,4},{24,8},{28,12},{1,17},{... | collective-permute-start | bytes 393224 | tf_op jit(solution)/shard_map/ppermute | solution.py:20
  108.6 7.7 %collective-permute-start.40 = (bf16[256,512]{1,0:T(8,128)(2,1)S(1)}, bf16[256,512]{1,0:T(8,128)(2,1)}, u32[]{:S(2)}, u32[]{:S(2)}) collective-permute-start(bf16[256,512]{1,0:T(8,128)(2,1)S(1)} %shard_map.217.refs_0_), channel_id=1, source_target_pairs={{0,8},{4,12},{8,0},{12,4},{16,24},{20,28},{24,16},{28,20},{1,9},{5... | collective-permute-start | bytes 786440 | tf_op jit(solution)/shard_map/ppermute | solution.py:20
  108.7 24.7 %collective-permute-start.38 = (bf16[8,80,256]{2,1,0:T(8,128)(2,1)S(1)}, bf16[8,80,256]{2,1,0:T(8,128)(2,1)S(1)}, u32[]{:S(2)}, u32[]{:S(2)}) collective-permute-start(bf16[8,80,256]{2,1,0:T(8,128)(2,1)S(1)} %all-to-all-done.own_ref.got_ref), channel_id=1, source_target_pairs={{0,1},{1,0},{2,3},{3,2},{4,5},{5,4},{6,7},{7,6},{8,9},{9,8},{10,11... | collective-permute-start | bytes 983048 | tf_op jit(solution)/shard_map/ppermute | solution.py:20
  108.8 24.6 %collective-permute-start.41 = (bf16[256,512]{1,0:T(8,128)(2,1)S(1)}, bf16[256,512]{1,0:T(8,128)(2,1)S(1)}, u32[]{:S(2)}, u32[]{:S(2)}) collective-permute-start(bf16[256,512]{1,0:T(8,128)(2,1)S(1)} %shard_map.217.refs_0_), channel_id=1, source_target_pairs={{0,4},{4,0},{8,12},{12,8},{16,20},{20,16},{24,28},{28,24},{1,5},{5... | collective-permute-start | bytes 786440 | tf_op jit(solution)/shard_map/ppermute | solution.py:20
  116.3 17.2 %collective-permute-start.42 = (bf16[256,512]{1,0:T(8,128)(2,1)}, bf16[256,512]{1,0:T(8,128)(2,1)S(1)}, u32[]{:S(2)}, u32[]{:S(2)}) collective-permute-start(bf16[256,512]{1,0:T(8,128)(2,1)} %collective-permute-done.40.refs_1_), channel_id=1, source_target_pairs={{0,4},{4,0},{8,12},{12,8},{16,20},{20,16},{24,28},{28,24},{1,5},{5... | collective-permute-start | bytes 786440 | tf_op jit(solution)/shard_map/ppermute | solution.py:20
  (64 other events, 488.1 us)
